TPU v7x, 32 devices: a whole 2x2x4 slice. The times are simulated.
32 devices in a mesh: sp: 16 (over z, y, x), tp: 2 (over core).
Axes of the slice: x: 2, y: 2, z: 4, core: 2. Of those that a mesh axis runs over, the one named last changes fastest.
Arguments:
- tokens: bfloat16 [8192, 3072], P('sp'), may hold values from -72 to 72
- w_query: bfloat16 [3072, 1024], P('sp', 'tp'), may hold values from -0.109375 to 0.109375
- w_key: bfloat16 [3072, 1024], P('sp', 'tp'), may hold values from -0.109375 to 0.109375
- w_value: bfloat16 [3072, 1024], P('sp', 'tp'), may hold values from -0.4375 to 0.4375
- w_out: bfloat16 [1024, 3072], P('tp', 'sp'), may hold values from -0.1875 to 0.1875
Outputs:
- mixed: bfloat16 [8192, 3072], P(('sp', 'tp'))
- row_lse: float32 [16, 8192], P('tp', 'sp')
All inputs are finite; a program needn't handle non-finite values.
Results may differ from a plain program's by a relative error of at most 0.014.
Values may be sent and summed in bfloat16 or wider, within the bound.
A program may use at most 64 MiB of HBM per device.

v0:
```python
import functools

import jax
import jax.numpy as jnp
from jax import lax
from jax.experimental import pallas as pl
from jax.experimental.pallas import tpu as pltpu
from jax.sharding import PartitionSpec as P

HEAD_SIZE = 64
KEYS_BEHIND = 128
LANES = 128

dilation_rates = (1, 4, 16)
neg_big = -1e30

MESH = pl.DeviceIdType.MESH
VMEM = pltpu.VMEM


def at(sp, tp):
    return {"sp": sp, "tp": tp}


def project_kernel(
    n, n_tp, group, far, wq_ref, wk_ref, wv_ref, tok_ref, o_ref, q_ref, kv_ref, halo_ref, o_plane, o_far,
    tok_all, w_all, w_ref, pack_sem, w1_send, w1_recv, up_send, up_recv, down_send, down_recv,
    t_send, t_recv, d_send, d_recv, f_send, f_recv, h_send, h_recv, o_send, o_recv, z_send, z_recv, own_sem,
):
    sp, tp = lax.axis_index("sp"), lax.axis_index("tp")
    planes = n // group
    g, plane = lax.rem(sp, group), sp // group
    rows = tok_ref.shape[0]
    part = rows // n_tp
    half = part // 2

    barrier = pltpu.get_barrier_semaphore()

    def greet(j, _):
        pl.semaphore_signal(barrier, inc=1, device_id=at(lax.rem(sp + j, n), tp), device_id_type=MESH)
        return _

    lax.fori_loop(1, n, greet, 0)
    for j in range(1, n_tp):
        pl.semaphore_signal(barrier, inc=1, device_id=at(sp, lax.rem(tp + j, n_tp)), device_id_type=MESH)

    own_t = pltpu.make_async_copy(tok_ref, tok_all.at[g], own_sem.at[0])
    own_o = pltpu.make_async_copy(o_ref, o_plane.at[g], own_sem.at[1])

    def pack(t, i):
        source = (wq_ref, wk_ref, wv_ref)[t].at[:, pl.ds(pl.multiple_of((g ^ i) * LANES, LANES), LANES)]
        lanes = pl.ds(t * LANES, LANES)
        to = w_all.at[sp, :, lanes] if i == 0 else w_ref.at[i, :, lanes]
        return pltpu.make_async_copy(source, to, pack_sem.at[t, i])

    for i in list(range(1, group)) + [0]:
        for t in range(3):
            pack(t, i).start()
    own_t.start()
    own_o.start()
    pl.semaphore_wait(barrier, n - 1 + n_tp - 1)

    def mate(i):
        return plane * group + (g ^ i)

    def w_in_plane(i):
        return pltpu.make_async_remote_copy(
            src_ref=w_ref.at[i], dst_ref=w_all.at[sp], send_sem=w1_send.at[i], recv_sem=w1_recv.at[i],
            device_id=at(mate(i), tp), device_id_type=MESH)

    def w_in_plane_arrives(i):
        return pltpu.make_async_remote_copy(
            src_ref=w_ref.at[i], dst_ref=w_all.at[mate(i)], send_sem=w1_send.at[i], recv_sem=w1_recv.at[i],
            device_id=at(mate(i), tp), device_id_type=MESH)

    def slab(p, i):
        return w_all.at[lax.rem(p + 2 * planes, planes) * group + (g ^ i)]

    def up(i, k, p):
        return pltpu.make_async_remote_copy(
            src_ref=slab(p, i), dst_ref=slab(p, i), send_sem=up_send.at[i, k], recv_sem=up_recv.at[i, k],
            device_id=at(lax.rem(sp + group, n), tp), device_id_type=MESH)

    def down(i, k, p):
        return pltpu.make_async_remote_copy(
            src_ref=slab(p, i), dst_ref=slab(p, i), send_sem=down_send.at[i, k], recv_sem=down_recv.at[i, k],
            device_id=at(lax.rem(sp + n - group, n), tp), device_id_type=MESH)

    def when(condition, action):
        @pl.when(condition)
        def _():
            action()

    first, last = plane == 0, plane == planes - 1

    def relay(k, i):
        when(~last & (plane - k + 1 >= 0), lambda: up(i, k, plane - k + 1).start())
        when(~first & (plane + k - 1 < planes), lambda: down(i, k, plane + k - 1).start())

    def relayed(k, i):
        when(plane - k >= 0, lambda: up(i, k, plane - k).wait_recv())
        when(plane + k < planes, lambda: down(i, k, plane + k).wait_recv())

    def relay_left(k, i):
        when(~last & (plane - k + 1 >= 0), lambda: up(i, k, plane - k + 1).wait_send())
        when(~first & (plane + k - 1 < planes), lambda: down(i, k, plane + k - 1).wait_send())

    def hops(body):
        def one(k, _):
            for i in range(group):
                body(k, i)
            return _

        return one

    def o_out(i):
        return pltpu.make_async_remote_copy(
            src_ref=o_ref, dst_ref=o_plane.at[g], send_sem=o_send.at[i], recv_sem=o_recv.at[i],
            device_id=at(mate(i), tp), device_id_type=MESH)

    def o_in(i):
        return pltpu.make_async_remote_copy(
            src_ref=o_ref, dst_ref=o_plane.at[g ^ i], send_sem=o_send.at[i], recv_sem=o_recv.at[i],
            device_id=at(mate(i), tp), device_id_type=MESH)

    mine = pl.ds(pl.multiple_of(tp * part, part), part)

    def halves(k):
        return pl.ds(pl.multiple_of(tp * part + k * half, half), half)

    def tokens_out(i):
        return pltpu.make_async_remote_copy(
            src_ref=tok_ref.at[mine], dst_ref=tok_all.at[g, mine], send_sem=t_send.at[i], recv_sem=t_recv.at[i],
            device_id=at(mate(i), tp), device_id_type=MESH)

    def tokens_in(i):
        return pltpu.make_async_remote_copy(
            src_ref=tok_ref.at[mine], dst_ref=tok_all.at[g ^ i, mine], send_sem=t_send.at[i], recv_sem=t_recv.at[i],
            device_id=at(mate(i), tp), device_id_type=MESH)

    def corner_out(i):
        ref = tok_all.at[g ^ i, halves(i - 1)]
        return pltpu.make_async_remote_copy(
            src_ref=ref, dst_ref=ref, send_sem=d_send.at[i], recv_sem=d_recv.at[i],
            device_id=at(mate(3 - i), tp), device_id_type=MESH)

    def corner_in(i):
        ref = tok_all.at[g ^ 3, halves(i - 1)]
        return pltpu.make_async_remote_copy(
            src_ref=ref, dst_ref=ref, send_sem=d_send.at[i], recv_sem=d_recv.at[i],
            device_id=at(mate(3 - i), tp), device_id_type=MESH)

    def across(i, j):
        ref = tok_all.at[g ^ i, mine]
        return pltpu.make_async_remote_copy(
            src_ref=ref, dst_ref=ref, send_sem=f_send.at[i, j], recv_sem=f_recv.at[i, j],
            device_id=at(sp, lax.rem(tp + j, n_tp)), device_id_type=MESH)

    def across_in(i, j):
        origin = lax.rem(tp + n_tp - j, n_tp)
        ref = tok_all.at[g ^ i, pl.ds(pl.multiple_of(origin * part, part), part)]
        return pltpu.make_async_remote_copy(
            src_ref=ref, dst_ref=ref, send_sem=f_send.at[i, j], recv_sem=f_recv.at[i, j],
            device_id=at(sp, lax.rem(tp + j, n_tp)), device_id_type=MESH)

    near = [i for i in (1, 2) if i < group]
    def z_out(k):
        return pltpu.make_async_remote_copy(
            src_ref=o_ref, dst_ref=o_far.at[k], send_sem=z_send.at[k], recv_sem=z_recv.at[k],
            device_id=at(lax.rem(sp + k * group, n), tp), device_id_type=MESH)

    for i in range(1, group):
        for t in range(3):
            pack(t, i).wait()
        w_in_plane(i).start()
    for t in range(3):
        pack(t, 0).wait()
    if planes > 1:
        relay(1, 0)
    for i in near:
        tokens_out(i).start()
    for i in range(1, group):
        w_in_plane_arrives(i).wait_recv()
        if planes > 1:
            relay(1, i)

    def pass_on(k, i):
        relayed(k, i)
        relay(k + 1, i)

    if planes > 1:
        lax.fori_loop(1, planes, lambda k, _: (z_out(k).start(), _)[1], 0)
        lax.fori_loop(1, planes - 1, hops(pass_on), 0)
    for i in near:
        tokens_in(i).wait_recv()
        if group == 4:
            corner_out(i).start()
        for j in range(1, n_tp):
            across(i, j).start()
    for i in range(1, group):
        o_out(i).start()
    if planes > 1:
        for i in range(group):
            relayed(planes - 1, i)
    own_t.wait()

    def halo_out(h, i):
        view = pl.ds(pl.multiple_of((g ^ i) * rows, rows), rows)
        return pltpu.make_async_remote_copy(
            src_ref=kv_ref.at[view], dst_ref=halo_ref.at[far - h, view],
            send_sem=h_send.at[h, i], recv_sem=h_recv.at[h, i],
            device_id=at(lax.rem(sp + h * group, n), tp), device_id_type=MESH)

    tile = min(256, rows)

    for i in range(group):
        if i == 3:
            for k in (1, 2):
                corner_in(k).wait_recv()
            for j in range(1, n_tp):
                across(i, j).start()
        if i > 0:
            for j in range(1, n_tp):
                across_in(i, j).wait_recv()
        block = g ^ i

        def one(s, _, block=block):
            x = tok_all[block, pl.ds(pl.multiple_of(s * tile, tile), tile), :]
            w = w_all[...].reshape(-1, 3 * LANES)
            y = jnp.dot(x, w, preferred_element_type=jnp.float32).astype(jnp.bfloat16)
            to = pl.ds(pl.multiple_of(block * rows + s * tile, tile), tile)
            q_ref[to, :] = y[:, :LANES]
            kv_ref[to, :] = y[:, LANES:]
            return _

        lax.fori_loop(0, rows // tile, one, 0)
        for h in range(1, far + 1):
            @pl.when(plane + h < planes)
            def _():
                halo_out(h, i).start()

    for h in range(1, far + 1):
        @pl.when(plane - h >= 0)
        def _():
            for i in range(group):
                halo_out(h, i).wait_recv()

        @pl.when(plane - h < 0)
        def _():
            halo_ref[far - h] = jnp.zeros(halo_ref.shape[1:], halo_ref.dtype)

        @pl.when(plane + h < planes)
        def _():
            for i in range(group):
                halo_out(h, i).wait_send()

    for i in range(1, group):
        w_in_plane(i).wait_send()
        for j in range(1, n_tp):
            across(i, j).wait_send()
    for i in near:
        tokens_out(i).wait_send()
        if group == 4:
            corner_out(i).wait_send()
    if planes > 1:
        lax.fori_loop(1, planes, hops(relay_left), 0)
        lax.fori_loop(1, planes, lambda k, _: (z_out(k).wait(), _)[1], 0)
    own_o.wait()
    for i in range(1, group):
        o_in(i).wait_recv()
        o_out(i).wait_send()


def attend_kernel(
    n, n_tp, group, heads, q_ref, kv_ref, halo_ref, o_far, o_plane, mixed_ref, lse_all,
    qs, ks, vs, top_s, den_s, acc_s, att, lse_ref, o_all, att_all, sums, sums_in,
    z_recv, b_send, b_recv, c_send, c_recv, a_send, a_recv, l_send, l_recv, s_send, s_recv, own_sem, o_sem,
):
    sp, tp = lax.axis_index("sp"), lax.axis_index("tp")
    planes = n // group
    g, plane = lax.rem(sp, group), sp // group
    own = q_ref.shape[0]
    base = plane * own
    rows = lse_all.shape[2]
    part = mixed_ref.shape[0]
    cut, width = o_plane.shape[1:]
    half = cut // 2

    def mate(i):
        return plane * group + (g ^ i)

    barrier = pltpu.get_barrier_semaphore()

    for i in range(1, group):
        pl.semaphore_signal(barrier, inc=1, device_id=at(mate(i), tp), device_id_type=MESH)
    for j in range(1, n_tp):
        pl.semaphore_signal(barrier, inc=1, device_id=at(sp, lax.rem(tp + j, n_tp)), device_id_type=MESH)

    def strip(k, i, part_of=None):
        origin = lax.rem(plane + planes - k, planes) * group + (g ^ i)
        if part_of is None:
            return o_all.at[pl.ds(pl.multiple_of(origin * cut, cut), cut)]
        return o_all.at[pl.ds(pl.multiple_of(origin * cut + part_of * half, half), half)]

    def z_in(k):
        return pltpu.make_async_copy(o_far.at[k], strip(k, 0), z_recv.at[k])

    def side_out(k, i):
        return pltpu.make_async_remote_copy(
            src_ref=o_far.at[k], dst_ref=strip(k, 0), send_sem=b_send.at[k, i], recv_sem=b_recv.at[k, i],
            device_id=at(mate(i), tp), device_id_type=MESH)

    def side_in(k, i):
        return pltpu.make_async_remote_copy(
            src_ref=strip(k, i), dst_ref=strip(k, i), send_sem=b_send.at[k, i], recv_sem=b_recv.at[k, i],
            device_id=at(mate(i), tp), device_id_type=MESH)

    def corner_out(k, i):
        return pltpu.make_async_remote_copy(
            src_ref=strip(k, i, i - 1), dst_ref=strip(k, i, i - 1), send_sem=c_send.at[k, i], recv_sem=c_recv.at[k, i],
            device_id=at(mate(3 - i), tp), device_id_type=MESH)

    def corner_in(k, i):
        return pltpu.make_async_remote_copy(
            src_ref=strip(k, 3, i - 1), dst_ref=strip(k, 3, i - 1), send_sem=c_send.at[k, i], recv_sem=c_recv.at[k, i],
            device_id=at(mate(3 - i), tp), device_id_type=MESH)

    near = [i for i in (1, 2) if i < group]

    def sides(k):
        for i in near:
            side_out(k, i).start()

    def corners(k):
        for i in near:
            side_in(k, i).wait_recv()
            if group == 4:
                corner_out(k, i).start()

    def settled(i):
        return pltpu.make_async_copy(o_plane.at[g ^ i], strip(0, i), o_sem.at[i])

    for i in range(group):
        settled(i).start()
    if planes > 1:
        lax.fori_loop(1, planes, lambda k, _: (z_in(k).start(), _)[1], 0)
    pl.semaphore_wait(barrier, group - 1 + n_tp - 1)
    if group > 1:
        for k in range(1, planes):
            sides(k)

    behind = ks.shape[0] - own
    pieces, piece_rows = halo_ref.shape[0], halo_ref.shape[1]
    qs[...] = q_ref[...].astype(jnp.float32) * HEAD_SIZE ** (-0.5)
    for h in range(pieces):
        ks[h * piece_rows : (h + 1) * piece_rows] = halo_ref[h, :, :LANES].astype(jnp.float32)
        vs[h * piece_rows : (h + 1) * piece_rows] = halo_ref[h, :, LANES:].astype(jnp.float32)
    ks[behind:] = kv_ref[:, :LANES].astype(jnp.float32)
    vs[behind:] = kv_ref[:, LANES:].astype(jnp.float32)

    passed = 0
    for number, d in enumerate(dilation_rates):
        step = min(KEYS_BEHIND, own // d)
        count = own // d // step
        span = step + KEYS_BEHIND

        def block(index, _, number=number, d=d, step=step, span=span):
            cls, b = lax.rem(index, d), index // d
            start = b * (step * d) + cls
            q_at = pl.ds(start, step, stride=d) if d > 1 else pl.ds(pl.multiple_of(start, step), step)
            k_start = behind - KEYS_BEHIND * d + start
            k_at = pl.ds(k_start, span, stride=d) if d > 1 else pl.ds(pl.multiple_of(k_start, step), span)
            q = qs[q_at, :]
            k = ks[k_at, :].astype(jnp.bfloat16)
            v = vs[k_at, :].astype(jnp.bfloat16)
            low = lax.broadcasted_iota(jnp.int32, (step, LANES), 1) < HEAD_SIZE
            q2 = jnp.concatenate([jnp.where(low, q, 0.0), jnp.where(low, 0.0, q)], axis=0).astype(jnp.bfloat16)
            s = lax.dot_general(q2, k, (((1,), (1,)), ((), ())), preferred_element_type=jnp.float32)
            row = lax.broadcasted_iota(jnp.int32, (step, span), 0)
            col = lax.broadcasted_iota(jnp.int32, (step, span), 1)
            dist = KEYS_BEHIND + row - col
            first = base // d + b * step - KEYS_BEHIND
            seen = (dist >= 0) & (dist <= KEYS_BEHIND) & (first + col >= 0)
            s = jnp.where(jnp.concatenate([seen, seen], axis=0), s, neg_big)
            top = jnp.max(s, axis=1, keepdims=True)
            p = jnp.exp(s - top)
            den = jnp.sum(p, axis=1, keepdims=True)
            o = jnp.dot(p.astype(jnp.bfloat16), v, preferred_element_type=jnp.float32)
            top = jnp.where(low, top[:step], top[step:])
            den = jnp.where(low, den[:step], den[step:])
            o = jnp.where(low, o[:step], o[step:])
            if number == 0:
                top_s[q_at, :] = top
                den_s[q_at, :] = den
                acc_s[q_at, :] = o
            else:
                was = top_s[q_at, :]
                new = jnp.maximum(was, top)
                old_scale, scale = jnp.exp(was - new), jnp.exp(top - new)
                top_s[q_at, :] = new
                den_s[q_at, :] = den_s[q_at, :] * old_scale + den * scale
                acc_s[q_at, :] = acc_s[q_at, :] * old_scale + o * scale
            return _

        lax.fori_loop(0, d * count, block, 0, unroll=2)
        if number + 1 < len(dilation_rates) and passed + 1 < planes:
            passed += 1
            corners(passed)

    att[...] = (acc_s[...] / den_s[...]).astype(jnp.bfloat16)

    def att_out(i):
        mine = pl.ds(pl.multiple_of((g ^ i) * rows, rows), rows)
        return pltpu.make_async_remote_copy(
            src_ref=att.at[mine], dst_ref=att_all.at[g], send_sem=a_send.at[i], recv_sem=a_recv.at[i],
            device_id=at(mate(i), tp), device_id_type=MESH)

    def att_in(i):
        return pltpu.make_async_remote_copy(
            src_ref=att.at[pl.ds(0, rows)], dst_ref=att_all.at[g ^ i], send_sem=a_send.at[i], recv_sem=a_recv.at[i],
            device_id=at(mate(i), tp), device_id_type=MESH)

    def lse_out(i):
        return pltpu.make_async_remote_copy(
            src_ref=lse_ref.at[g ^ i], dst_ref=lse_all.at[g], send_sem=l_send.at[i], recv_sem=l_recv.at[i],
            device_id=at(mate(i), tp), device_id_type=MESH)

    def lse_in(i):
        return pltpu.make_async_remote_copy(
            src_ref=lse_ref.at[g ^ i], dst_ref=lse_all.at[g ^ i], send_sem=l_send.at[i], recv_sem=l_recv.at[i],
            device_id=at(mate(i), tp), device_id_type=MESH)

    for i in range(1, group):
        att_out(i).start()
    own_a = pltpu.make_async_copy(att.at[pl.ds(pl.multiple_of(g * rows, rows), rows)], att_all.at[g], own_sem.at[1])
    own_a.start()

    for t in range(own // LANES):
        at_rows = pl.ds(t * LANES, LANES)
        lse = (top_s[at_rows, :] + jnp.log(den_s[at_rows, :])).T
        b, off = (t * LANES) // rows, (t * LANES) % rows
        for h in range(heads):
            lse_ref[b, h : h + 1, off : off + LANES] = lse[h * HEAD_SIZE : h * HEAD_SIZE + 1, :]
    for i in range(1, group):
        lse_out(i).start()
    own_l = pltpu.make_async_copy(lse_ref.at[g], lse_all.at[g], own_sem.at[2])
    own_l.start()

    while group > 1 and passed + 1 < planes:
        passed += 1
        corners(passed)
    if planes > 1:
        lax.fori_loop(1, planes, lambda k, _: (z_in(k).wait(), _)[1], 0)
    for i in range(group):
        settled(i).wait()
    own_a.wait()
    for i in range(1, group):
        att_in(i).wait_recv()

    chunks, chunk = sums.shape[1], sums.shape[3]
    by_plane = group > 1

    def columns_of(k):
        if by_plane:
            c = lax.rem(plane + planes - k, planes)
            return pl.ds(pl.multiple_of(c * chunk, chunk), chunk)
        return pl.ds(k * chunk, chunk)

    def product(c, j):
        wanted = lax.rem(tp + j, n_tp)
        here = pl.ds(pl.multiple_of(wanted * part, part), part)
        a = jnp.concatenate([att_all[b, here, :] for b in range(group)], axis=1)
        w = o_all[columns_of(c), :]
        return lax.dot_general(a, w, (((1,), (1,)), ((), ())), preferred_element_type=jnp.float32)

    def sum_out(c, j):
        return pltpu.make_async_remote_copy(
            src_ref=sums.at[j, c], dst_ref=sums_in.at[j, c], send_sem=s_send.at[j, c], recv_sem=s_recv.at[j, c],
            device_id=at(sp, lax.rem(tp + j, n_tp)), device_id_type=MESH)

    def for_others(c):
        for j in range(1, n_tp):
            sums[j, c] = product(c, j).astype(jnp.bfloat16)
            sum_out(c, j).start()

    def for_self(c):
        total = product(c, 0).astype(jnp.bfloat16).astype(jnp.float32)
        for j in range(1, n_tp):
            sum_out(c, j).wait_recv()
            total += sums_in[j, c].astype(jnp.float32)
        mixed_ref[:, columns_of(c)] = total.astype(jnp.bfloat16)

    for c in range(chunks):
        if group == 4 and c > 0:
            for i in near:
                corner_in(c, i).wait_recv()
        for_others(c)
        if 0 < c < chunks - 1:
            for_self(c - 1)
    if chunks > 1:
        for_self(chunks - 2)
    for_self(chunks - 1)

    own_l.wait()
    for i in range(1, group):
        lse_in(i).wait_recv()
    for j in range(1, n_tp):
        for c in range(chunks):
            sum_out(c, j).wait_send()
    for i in range(1, group):
        att_out(i).wait_send()
        lse_out(i).wait_send()
    if group > 1:
        for k in range(1, planes):
            for i in near:
                side_out(k, i).wait_send()
                if group == 4:
                    corner_out(k, i).wait_send()


def shards(n, n_tp, tokens, w_query, w_key, w_value, w_out):
    rows, model = tokens.shape
    depth, width = w_query.shape
    slabs = width // LANES
    reach = KEYS_BEHIND * dilation_rates[-1]
    group = 1
    while group < 4 and group * rows < reach and slabs % (2 * group) == 0 and n % (2 * group) == 0:
        group *= 2
    assert slabs == group
    far = (reach + group * rows - 1) // (group * rows)
    planes = n // group
    own = group * rows
    part = rows // n_tp
    heads = LANES // HEAD_SIZE

    turned = w_out.T
    cut = w_out.shape[1]

    dma = pltpu.SemaphoreType.DMA
    vmem = pl.BlockSpec(memory_space=VMEM)
    q, kv, halo, o_plane, o_far = pl.pallas_call(
        functools.partial(project_kernel, n, n_tp, group, far),
        out_shape=(
            jax.ShapeDtypeStruct((own, LANES), jnp.bfloat16),
            jax.ShapeDtypeStruct((own, 2 * LANES), jnp.bfloat16),
            jax.ShapeDtypeStruct((far, own, 2 * LANES), jnp.bfloat16),
            jax.ShapeDtypeStruct((group, cut, width), jnp.bfloat16),
            jax.ShapeDtypeStruct((planes, cut, width), jnp.bfloat16),
        ),
        in_specs=[pl.BlockSpec(memory_space=pltpu.HBM)] * 4 + [vmem],
        out_specs=(vmem,) * 5,
        scratch_shapes=[
            VMEM((group, rows, model), jnp.bfloat16),
            VMEM((n, depth, 3 * LANES), jnp.bfloat16),
            VMEM((group, depth, 3 * LANES), jnp.bfloat16),
            dma((3, group)),
            dma((group,)), dma((group,)),
            dma((group, planes)), dma((group, planes)),
            dma((group, planes)), dma((group, planes)),
            dma((group,)), dma((group,)),
            dma((group,)), dma((group,)),
            dma((group, n_tp)), dma((group, n_tp)),
            dma((far + 1, group)), dma((far + 1, group)),
            dma((group,)), dma((group,)), dma((planes,)), dma((planes,)),
            dma((2,)),
        ],
        compiler_params=pltpu.CompilerParams(collective_id=0, has_side_effects=True, vmem_limit_bytes=48 << 20),
        cost_estimate=pl.CostEstimate(flops=2 * own * model * 3 * LANES, bytes_accessed=1 << 24, transcendentals=0),
        name="project",
    )(w_query, w_key, w_value, tokens, turned)

    behind = far * own
    f32, bf16 = jnp.float32, jnp.bfloat16
    chunks = planes if group > 1 else (4 if (n * cut) % (4 * LANES) == 0 else 1)
    chunk = n * cut // chunks
    return_shapes = (
        jax.ShapeDtypeStruct((part, n * cut), bf16),
        jax.ShapeDtypeStruct((group, heads, rows), f32),
    )
    mixed, lse = pl.pallas_call(
        functools.partial(attend_kernel, n, n_tp, group, heads),
        out_shape=return_shapes,
        in_specs=[vmem] * 5,
        out_specs=(vmem, vmem),
        scratch_shapes=[
            VMEM((own, LANES), f32), VMEM((behind + own, LANES), f32), VMEM((behind + own, LANES), f32),
            VMEM((own, LANES), f32), VMEM((own, LANES), f32), VMEM((own, LANES), f32),
            VMEM((own, LANES), bf16), VMEM((group, heads, rows), f32),
            VMEM((n * cut, width), bf16), VMEM((group, rows, LANES), bf16),
            VMEM((n_tp, chunks, part, chunk), bf16), VMEM((n_tp, chunks, part, chunk), bf16),
            dma((planes,)),
            dma((planes, group)), dma((planes, group)),
            dma((planes, group)), dma((planes, group)),
            dma((group,)), dma((group,)), dma((group,)), dma((group,)),
            dma((n_tp, chunks)), dma((n_tp, chunks)),
            dma((3,)), dma((group,)),
        ],
        compiler_params=pltpu.CompilerParams(collective_id=1, has_side_effects=True, vmem_limit_bytes=48 << 20),
        cost_estimate=pl.CostEstimate(flops=1 << 32, bytes_accessed=1 << 22, transcendentals=1 << 22),
        name="attend",
    )(q, kv, halo, o_far, o_plane)
    return mixed, lse.reshape(group * heads, rows)


def solution(mesh):
    placed = (P("sp", None), P("sp", "tp"), P("sp", "tp"), P("sp", "tp"), P("tp", "sp"))
    return jax.shard_map(
        functools.partial(shards, mesh.shape["sp"], mesh.shape["tp"]),
        mesh=mesh,
        in_specs=placed,
        out_specs=(P(("sp", "tp"), None), P("tp", "sp")),
        check_vma=False,
    )
```

profile of v0, /device:TPU:0, one launch (start us, length us, event | category | flops | bytes accessed | tf_op | source)
XLA Modules:
  0.0 123.8 jit_solution(18357020382565554043)
XLA Ops:
  0.6 0.0 copy-start
  0.6 0.9 copy-done
  1.6 0.0 copy-start.1
  1.6 0.9 copy-done.1
  2.5 0.0 copy-start.2
  2.5 0.9 copy-done.2
  3.4 0.0 copy-start.3
  3.4 0.9 copy-done.3
  4.3 82.4 %project.1 = (bf16[2048,128]{1,0:T(8,128)(2,1)S(1)}, bf16[2048,256]{1,0:T(8,128)(2,1)S(1)}, bf16[1,2048,256]{2,1,0:T(8,128)(2,1)S(1)}, bf16[4,192,512]{2,1,0:T(8,128)(2,1)S(1)}, bf16[4,192,512]{2,1,0:T(8,128)(2,1)S(1)}) custom-call(bf16[192,512]{1,0:T(8,128)(2,1)S(1)} %copy-done, bf16[192,512]{1,0:T(8,128)(2,1)S(1)} %copy-done.1, ...), custom_call_target="tpu_custom_call" | custom-call | flops 4831838208 | bytes 16777216 | tf_op jit(solution)/shard_map/project/pallas_call | solution.py:541
  86.8 35.2 %attend.1 = (bf16[256,3072]{1,0:T(8,128)(2,1)S(1)}, f32[4,2,512]{2,1,0:T(2,128)S(1)}) custom-call(bf16[2048,128]{1,0:T(8,128)(2,1)S(1)} %get-tuple-element.9.q_ref, bf16[2048,256]{1,0:T(8,128)(2,1)S(1)} %get-tuple-element.10.kv_ref, bf16[1,2048,256]{2,1,0:T(8,128)(2,1)S(1)} %get-tuple-element.11.halo_ref, bf16[4,192,512]{2,1,0:T(8,128)(2,1)S(1)} %get-tuple-element.12.o_far, ...), custom_call_target="tpu_custom_call" | custom-call | flops 4294967296 | bytes 4194304 | tf_op jit(solution)/shard_map/attend/pallas_call | solution.py:580
  122.0 0.6 reshape.7
  122.6 1.1 copy.8
Async XLA Ops:
  0.6 0.9 copy-start
  1.6 0.9 copy-start.1
  2.5 0.9 copy-start.2
  3.4 0.9 copy-start.3
where the time goes:
time: 124 us
  Pallas kernels  118 us (95%)
  local copies, waits for them, and re-layouts  5.46 us (4%)
    pallas_call x1, Pallas kernels, shards(): pl.pallas_call(functools.partial(project_kernel, n, n_tp, group, far), ou...  82.4 us
    pallas_call x1, Pallas kernels, shards(): pl.pallas_call(functools.partial(attend_kernel, n, n_tp, group, heads), o...  35.2 us
    unnamed x9, local copies, waits for them, and re-layouts  4.84 us

commit v1 on v0

v1 whole, which is shorter than its diff:
```python
import functools

import jax
import jax.numpy as jnp
from jax import lax
from jax.experimental import pallas as pl
from jax.experimental.pallas import tpu as pltpu
from jax.sharding import PartitionSpec as P

HEAD_SIZE = 64
KEYS_BEHIND = 128
LANES = 128

dilation_rates = (1, 4, 16)
neg_big = -1e30

MESH = pl.DeviceIdType.MESH
VMEM = pltpu.VMEM


def at(sp, tp):
    return {"sp": sp, "tp": tp}


def layer_kernel(
    n, n_tp, group, far, heads, wq_ref, wk_ref, wv_ref, tok_ref, o_ref, mixed_ref, lse_out_ref,
    tok_all, w_all, w_ref, kv_ref, halo_ref, o_all, qs, ks, vs, bias, top_s, den_s, acc_s, att, lse_ref, lse_all,
    att_all, sums, sums_in,
    pack_sem, own_sem, w1_send, w1_recv, up_send, up_recv, down_send, down_recv, t_send, t_recv, d_send, d_recv,
    f_send, f_recv, h_send, h_recv, ou_send, ou_recv, od_send, od_recv, b_send, b_recv, c_send, c_recv,
    a_send, a_recv, l_send, l_recv, s_send, s_recv,
):
    sp, tp = lax.axis_index("sp"), lax.axis_index("tp")
    planes = n // group
    g, plane = lax.rem(sp, group), sp // group
    rows = tok_ref.shape[0]
    own = group * rows
    base = plane * own
    half = rows // 2
    unit_rows = half // n_tp
    part = mixed_ref.shape[0]
    cut, width = o_ref.shape
    half_cut = cut // 2
    behind = far * own

    above = lax.rem(sp + group, n)
    below = lax.rem(sp + n - group, n)

    def mate(i):
        return plane * group + (g ^ i)

    near = [i for i in (1, 2) if i < group]

    barrier = pltpu.get_barrier_semaphore()
    greeted = 0

    def greet(sp_to, tp_to):
        pl.semaphore_signal(barrier, inc=1, device_id=at(sp_to, tp_to), device_id_type=MESH)
        return 1

    for i in range(1, group):
        greeted += greet(mate(i), tp)
    if planes > 1:
        for h in range(1, max(far, 1) + 1):
            greeted += greet(lax.rem(sp + h * group, n), tp)
            greeted += greet(lax.rem(sp + n - h * group, n), tp)
    for j in range(1, n_tp):
        greeted += greet(sp, lax.rem(tp + j, n_tp))

    own_t = pltpu.make_async_copy(tok_ref, tok_all.at[g], own_sem.at[0])

    def strip(q, i, part_of=None):
        origin = q * group + (g ^ i)
        if part_of is None:
            return o_all.at[pl.ds(pl.multiple_of(origin * cut, cut), cut)]
        return o_all.at[pl.ds(pl.multiple_of(origin * cut + part_of * half_cut, half_cut), half_cut)]

    own_o = pltpu.make_async_copy(o_ref, strip(plane, 0), own_sem.at[3])

    def pack(t, i):
        source = (wq_ref, wk_ref, wv_ref)[t].at[:, pl.ds(pl.multiple_of((g ^ i) * LANES, LANES), LANES)]
        lanes = pl.ds(t * LANES, LANES)
        to = w_all.at[sp, :, lanes] if i == 0 else w_ref.at[i, :, lanes]
        return pltpu.make_async_copy(source, to, pack_sem.at[t, i])

    for i in list(range(1, group)) + [0]:
        for t in range(3):
            pack(t, i).start()
    own_o.start()
    own_t.start()
    pl.semaphore_wait(barrier, greeted)

    def w_in_plane(i):
        return pltpu.make_async_remote_copy(
            src_ref=w_ref.at[i], dst_ref=w_all.at[sp], send_sem=w1_send.at[i], recv_sem=w1_recv.at[i],
            device_id=at(mate(i), tp), device_id_type=MESH)

    def w_in_plane_arrives(i):
        return pltpu.make_async_remote_copy(
            src_ref=w_ref.at[i], dst_ref=w_all.at[mate(i)], send_sem=w1_send.at[i], recv_sem=w1_recv.at[i],
            device_id=at(mate(i), tp), device_id_type=MESH)

    def slab(p, i):
        return w_all.at[lax.rem(p + 2 * planes, planes) * group + (g ^ i)]

    def up(i, k, p):
        return pltpu.make_async_remote_copy(
            src_ref=slab(p, i), dst_ref=slab(p, i), send_sem=up_send.at[i, k], recv_sem=up_recv.at[i, k],
            device_id=at(above, tp), device_id_type=MESH)

    def down(i, k, p):
        return pltpu.make_async_remote_copy(
            src_ref=slab(p, i), dst_ref=slab(p, i), send_sem=down_send.at[i, k], recv_sem=down_recv.at[i, k],
            device_id=at(below, tp), device_id_type=MESH)

    def o_up(k, p):
        ref = strip(lax.rem(p + 2 * planes, planes), 0)
        return pltpu.make_async_remote_copy(
            src_ref=ref, dst_ref=ref, send_sem=ou_send.at[k], recv_sem=ou_recv.at[k],
            device_id=at(above, tp), device_id_type=MESH)

    def o_down(k, p):
        ref = strip(lax.rem(p + 2 * planes, planes), 0)
        return pltpu.make_async_remote_copy(
            src_ref=ref, dst_ref=ref, send_sem=od_send.at[k], recv_sem=od_recv.at[k],
            device_id=at(below, tp), device_id_type=MESH)

    def when(condition, action):
        @pl.when(condition)
        def _():
            action()

    first, last = plane == 0, plane == planes - 1

    def relay(k, i):
        when(~last & (plane - k + 1 >= 0), lambda: up(i, k, plane - k + 1).start())
        when(~first & (plane + k - 1 < planes), lambda: down(i, k, plane + k - 1).start())

    def relayed(k, i):
        when(plane - k >= 0, lambda: up(i, k, plane - k).wait_recv())
        when(plane + k < planes, lambda: down(i, k, plane + k).wait_recv())

    def relay_left(k, i):
        when(~last & (plane - k + 1 >= 0), lambda: up(i, k, plane - k + 1).wait_send())
        when(~first & (plane + k - 1 < planes), lambda: down(i, k, plane + k - 1).wait_send())

    def o_relay(k):
        when(~last & (plane - k + 1 >= 0), lambda: o_up(k, plane - k + 1).start())
        when(~first & (plane + k - 1 < planes), lambda: o_down(k, plane + k - 1).start())

    def o_relay_left(k):
        when(~last & (plane - k + 1 >= 0), lambda: o_up(k, plane - k + 1).wait_send())
        when(~first & (plane + k - 1 < planes), lambda: o_down(k, plane + k - 1).wait_send())

    def hops(body):
        def one(k, _):
            for i in range(group):
                body(k, i)
            return _

        return one

    def back(q):
        return lax.rem(plane - q + planes, planes)

    def side_out(q, i):
        k = back(q)
        return pltpu.make_async_remote_copy(
            src_ref=strip(q, 0), dst_ref=strip(q, 0), send_sem=b_send.at[k, i], recv_sem=b_recv.at[k, i],
            device_id=at(mate(i), tp), device_id_type=MESH)

    def side_in(q, i):
        k = back(q)
        return pltpu.make_async_remote_copy(
            src_ref=strip(q, i), dst_ref=strip(q, i), send_sem=b_send.at[k, i], recv_sem=b_recv.at[k, i],
            device_id=at(mate(i), tp), device_id_type=MESH)

    def edge_out(q, i):
        k = back(q)
        return pltpu.make_async_remote_copy(
            src_ref=strip(q, i, i - 1), dst_ref=strip(q, i, i - 1), send_sem=c_send.at[k, i], recv_sem=c_recv.at[k, i],
            device_id=at(mate(3 - i), tp), device_id_type=MESH)

    def edge_in(q, i):
        k = back(q)
        return pltpu.make_async_remote_copy(
            src_ref=strip(q, 3, i - 1), dst_ref=strip(q, 3, i - 1), send_sem=c_send.at[k, i], recv_sem=c_recv.at[k, i],
            device_id=at(mate(3 - i), tp), device_id_type=MESH)

    def sides(q):
        for i in near:
            side_out(q, i).start()

    def edges(q):
        for i in near:
            side_in(q, i).wait_recv()
            if group == 4:
                edge_out(q, i).start()

    def o_relayed(k):
        def from_below():
            o_up(k, plane - k).wait_recv()

        def from_above():
            o_down(k, plane + k).wait_recv()

        when(plane - k >= 0, from_below)
        when(plane + k < planes, from_above)

    def o_sides(k):
        if near:
            when(plane - k >= 0, lambda: sides(plane - k))
            when(plane + k < planes, lambda: sides(plane + k))

    def unit(k, t):
        return pl.ds(pl.multiple_of(k * half + t * unit_rows, unit_rows), unit_rows)

    def tokens_out(i, k):
        return pltpu.make_async_remote_copy(
            src_ref=tok_ref.at[unit(k, tp)], dst_ref=tok_all.at[g, unit(k, tp)],
            send_sem=t_send.at[i, k], recv_sem=t_recv.at[i, k], device_id=at(mate(i), tp), device_id_type=MESH)

    def tokens_in(i, k):
        return pltpu.make_async_remote_copy(
            src_ref=tok_ref.at[unit(k, tp)], dst_ref=tok_all.at[g ^ i, unit(k, tp)],
            send_sem=t_send.at[i, k], recv_sem=t_recv.at[i, k], device_id=at(mate(i), tp), device_id_type=MESH)

    def corner_out(i):
        ref = tok_all.at[g ^ i, unit(i - 1, tp)]
        return pltpu.make_async_remote_copy(
            src_ref=ref, dst_ref=ref, send_sem=d_send.at[i], recv_sem=d_recv.at[i],
            device_id=at(mate(3 - i), tp), device_id_type=MESH)

    def corner_in(i):
        ref = tok_all.at[g ^ 3, unit(i - 1, tp)]
        return pltpu.make_async_remote_copy(
            src_ref=ref, dst_ref=ref, send_sem=d_send.at[i], recv_sem=d_recv.at[i],
            device_id=at(mate(3 - i), tp), device_id_type=MESH)

    def across(i, k, j):
        ref = tok_all.at[g ^ i, unit(k, tp)]
        return pltpu.make_async_remote_copy(
            src_ref=ref, dst_ref=ref, send_sem=f_send.at[i, k, j], recv_sem=f_recv.at[i, k, j],
            device_id=at(sp, lax.rem(tp + j, n_tp)), device_id_type=MESH)

    def across_in(i, k, j):
        ref = tok_all.at[g ^ i, unit(k, lax.rem(tp + n_tp - j, n_tp))]
        return pltpu.make_async_remote_copy(
            src_ref=ref, dst_ref=ref, send_sem=f_send.at[i, k, j], recv_sem=f_recv.at[i, k, j],
            device_id=at(sp, lax.rem(tp + j, n_tp)), device_id_type=MESH)

    def to_other_cores(i, k):
        for j in range(1, n_tp):
            across(i, k, j).start()

    def piece(i, s):
        return s if i == 1 else 1 - s

    for i in range(1, group):
        for t in range(3):
            pack(t, i).wait()
        w_in_plane(i).start()
    for t in range(3):
        pack(t, 0).wait()
    if planes > 1:
        relay(1, 0)
    for s in range(2):
        for i in near:
            tokens_out(i, piece(i, s)).start()
    for i in range(1, group):
        w_in_plane_arrives(i).wait_recv()
        if planes > 1:
            relay(1, i)

    def pass_on(k, i):
        relayed(k, i)
        relay(k + 1, i)

    row = lax.broadcasted_iota(jnp.int32, (KEYS_BEHIND, 2 * KEYS_BEHIND), 0)
    col = lax.broadcasted_iota(jnp.int32, (KEYS_BEHIND, 2 * KEYS_BEHIND), 1)
    dist = KEYS_BEHIND + row - col
    band = (dist >= 0) & (dist <= KEYS_BEHIND)
    bias[0] = jnp.where(band, 0.0, neg_big)
    for number, d in enumerate(dilation_rates):
        bias[1 + number] = jnp.where(band & (base // d - KEYS_BEHIND + col >= 0), 0.0, neg_big)
    for h in range(1, far + 1):
        @pl.when(plane - h < 0)
        def _():
            ks[(far - h) * own : (far - h + 1) * own] = jnp.zeros((own, LANES), jnp.float32)
            vs[(far - h) * own : (far - h + 1) * own] = jnp.zeros((own, LANES), jnp.float32)

    if planes > 1:
        lax.fori_loop(1, planes - 1, hops(pass_on), 0)
    own_o.wait()
    if planes > 1:
        o_relay(1)
    for i in near:
        tokens_in(i, piece(i, 0)).wait_recv()
        if group == 4:
            corner_out(i).start()
        to_other_cores(i, piece(i, 0))
    if planes > 1:
        for i in range(group):
            relayed(planes - 1, i)
    for i in near:
        tokens_in(i, piece(i, 1)).wait_recv()
        to_other_cores(i, piece(i, 1))
    if near:
        sides(plane)
    own_t.wait()

    def halo_out(h, i, k):
        view = pl.ds(pl.multiple_of((g ^ i) * rows + k * half, half), half)
        return pltpu.make_async_remote_copy(
            src_ref=kv_ref.at[view], dst_ref=halo_ref.at[far - h, view],
            send_sem=h_send.at[h, i, k], recv_sem=h_recv.at[h, i, k],
            device_id=at(lax.rem(sp + h * group, n), tp), device_id_type=MESH)

    def tile(i, k):
        block = g ^ i
        x = tok_all[block, pl.ds(pl.multiple_of(k * half, half), half), :]
        w = w_all[...].reshape(-1, 3 * LANES)
        y = jnp.dot(x, w, preferred_element_type=jnp.float32).astype(jnp.bfloat16)
        start = block * rows + k * half
        to = pl.ds(pl.multiple_of(start, half), half)
        past = pl.ds(pl.multiple_of(behind + start, half), half)
        kv_ref[to, :] = y[:, LANES:]
        qs[to, :] = y[:, :LANES].astype(jnp.float32) * HEAD_SIZE ** (-0.5)
        ks[past, :] = y[:, LANES : 2 * LANES].astype(jnp.float32)
        vs[past, :] = y[:, 2 * LANES :].astype(jnp.float32)
        for h in range(1, far + 1):
            @pl.when(plane + h < planes)
            def _():
                halo_out(h, i, k).start()

    def tiles(picks, ready):
        def one(s, _):
            i, k = picks(s)
            ready(i, k)
            tile(i, k)
            return _

        lax.fori_loop(0, 2, one, 0)

    def crossed(i, k):
        for j in range(1, n_tp):
            across_in(i, k, j).wait_recv()

    def o_step(k):
        if k < planes:
            o_relayed(k)
            o_sides(k)
            if k + 1 < planes:
                o_relay(k + 1)

    tiles(lambda s: (0, s), lambda i, k: None)
    if group > 1:
        o_step(1)
    if group == 2:
        tiles(lambda s: (1, s), crossed)
    if group == 4:
        tiles(lambda s: (1 + s, s), crossed)
        o_step(2)
        tiles(lambda s: (1 + s, 1 - s), crossed)
        o_step(3)
        for k in (1, 2):
            corner_in(k).wait_recv()
            to_other_cores(3, k - 1)
        tiles(lambda s: (3, s), crossed)
    done = {1: 1, 2: 2, 4: 4}[group]

    def o_rest(k, _):
        o_relayed(k)
        o_sides(k)
        if True:
            when(k + 1 < planes, lambda: o_relay(k + 1))
        return _

    if done < planes:
        lax.fori_loop(done, planes, o_rest, 0)

    def nearest(m):
        left, right = plane, planes - 1 - plane
        short = jnp.minimum(left, right)
        zigzag = plane + (m // 2 if m % 2 == 0 else -((m + 1) // 2))
        return jnp.where(m <= 2 * short, zigzag, jnp.where(left < right, m, planes - 1 - m))

    by_plane = group > 1
    passed = 0

    def edges_next():
        nonlocal passed
        if by_plane and passed < planes:
            edges(nearest(passed))
            passed += 1

    low_of = {}

    def attention(number, begin, end, unroll):
        d = dilation_rates[number]
        step = min(KEYS_BEHIND, own // d)
        span = step + KEYS_BEHIND
        mask_at = 1 + number if begin == 0 else 0

        def block(index, _):
            cls, b = lax.rem(index, d), index // d
            start = b * (step * d) + cls
            q_at = pl.ds(start, step, stride=d) if d > 1 else pl.ds(pl.multiple_of(start, step), step)
            k_start = behind - KEYS_BEHIND * d + start
            k_at = pl.ds(k_start, span, stride=d) if d > 1 else pl.ds(pl.multiple_of(k_start, step), span)
            q = qs[q_at, :]
            k = ks[k_at, :].astype(jnp.bfloat16)
            v = vs[k_at, :].astype(jnp.bfloat16)
            v = jnp.concatenate([v, jnp.ones((span, LANES), jnp.bfloat16)], axis=1)
            low = lax.broadcasted_iota(jnp.int32, (step, LANES), 1) < HEAD_SIZE
            q2 = jnp.concatenate([jnp.where(low, q, 0.0), jnp.where(low, 0.0, q)], axis=0).astype(jnp.bfloat16)
            s = lax.dot_general(q2, k, (((1,), (1,)), ((), ())), preferred_element_type=jnp.float32)
            seen = bias[mask_at, :step, :span]
            s = s + jnp.concatenate([seen, seen], axis=0)
            top = jnp.max(s, axis=1, keepdims=True)
            p = jnp.exp(s - top)
            o = jnp.dot(p.astype(jnp.bfloat16), v, preferred_element_type=jnp.float32)
            top = jnp.where(low, top[:step], top[step:])
            den = jnp.where(low, o[:step, LANES:], o[step:, LANES:])
            o = jnp.where(low, o[:step, :LANES], o[step:, :LANES])
            if number == 0:
                top_s[q_at, :] = top
                den_s[q_at, :] = den
                acc_s[q_at, :] = o
            else:
                was = top_s[q_at, :]
                new = jnp.maximum(was, top)
                old_scale, scale = jnp.exp(was - new), jnp.exp(top - new)
                top_s[q_at, :] = new
                den_s[q_at, :] = den_s[q_at, :] * old_scale + den * scale
                acc_s[q_at, :] = acc_s[q_at, :] * old_scale + o * scale
            return _

        lax.fori_loop(begin * d, end * d, block, 0, unroll=unroll)

    counts = [own // d // min(KEYS_BEHIND, own // d) for d in dilation_rates]

    def unroll_of(trips):
        return next(u for u in (2, 3, 1) if trips % u == 0)

    for number, d in enumerate(dilation_rates):
        if counts[number] > 1:
            attention(number, 1, counts[number], unroll_of((counts[number] - 1) * d))
            edges_next()

    for h in range(1, far + 1):
        @pl.when(plane - h >= 0)
        def _():
            for i in range(group):
                for k in range(2):
                    halo_out(h, i, k).wait_recv()
            to = slice((far - h) * own, (far - h + 1) * own)
            ks[to] = halo_ref[far - h, :, :LANES].astype(jnp.float32)
            vs[to] = halo_ref[far - h, :, LANES:].astype(jnp.float32)

    for number, d in enumerate(dilation_rates):
        attention(number, 0, 1, unroll_of(d))
        edges_next()

    att[...] = (acc_s[...] / den_s[...]).astype(jnp.bfloat16)

    def att_out(i):
        mine = pl.ds(pl.multiple_of((g ^ i) * rows, rows), rows)
        return pltpu.make_async_remote_copy(
            src_ref=att.at[mine], dst_ref=att_all.at[g], send_sem=a_send.at[i], recv_sem=a_recv.at[i],
            device_id=at(mate(i), tp), device_id_type=MESH)

    def att_in(i):
        return pltpu.make_async_remote_copy(
            src_ref=att.at[pl.ds(0, rows)], dst_ref=att_all.at[g ^ i], send_sem=a_send.at[i], recv_sem=a_recv.at[i],
            device_id=at(mate(i), tp), device_id_type=MESH)

    def lse_out(i):
        return pltpu.make_async_remote_copy(
            src_ref=lse_ref.at[g ^ i], dst_ref=lse_all.at[g], send_sem=l_send.at[i], recv_sem=l_recv.at[i],
            device_id=at(mate(i), tp), device_id_type=MESH)

    def lse_in(i):
        return pltpu.make_async_remote_copy(
            src_ref=lse_ref.at[g ^ i], dst_ref=lse_all.at[g ^ i], send_sem=l_send.at[i], recv_sem=l_recv.at[i],
            device_id=at(mate(i), tp), device_id_type=MESH)

    for i in range(1, group):
        att_out(i).start()
    own_a = pltpu.make_async_copy(att.at[pl.ds(pl.multiple_of(g * rows, rows), rows)], att_all.at[g], own_sem.at[1])
    own_a.start()

    for t in range(own // LANES):
        at_rows = pl.ds(t * LANES, LANES)
        lse = (top_s[at_rows, :] + jnp.log(den_s[at_rows, :])).T
        b, off = (t * LANES) // rows, (t * LANES) % rows
        for h in range(heads):
            lse_ref[b, h : h + 1, off : off + LANES] = lse[h * HEAD_SIZE : h * HEAD_SIZE + 1, :]
    for i in range(1, group):
        lse_out(i).start()
    own_l = pltpu.make_async_copy(lse_ref.at[g], lse_all.at[g], own_sem.at[2])
    own_l.start()

    while by_plane and passed < planes:
        edges_next()
    own_a.wait()
    for i in range(1, group):
        att_in(i).wait_recv()

    chunks, chunk = sums.shape[1], sums.shape[3]

    def columns_of(m):
        if by_plane:
            return pl.ds(pl.multiple_of(nearest(m) * chunk, chunk), chunk)
        return pl.ds(m * chunk, chunk)

    def product(c, j):
        wanted = lax.rem(tp + j, n_tp)
        here = pl.ds(pl.multiple_of(wanted * part, part), part)
        a = jnp.concatenate([att_all[b, here, :] for b in range(group)], axis=1)
        w = o_all[columns_of(c), :]
        return lax.dot_general(a, w, (((1,), (1,)), ((), ())), preferred_element_type=jnp.float32)

    def sum_out(c, j):
        return pltpu.make_async_remote_copy(
            src_ref=sums.at[j, c], dst_ref=sums_in.at[j, c], send_sem=s_send.at[j, c], recv_sem=s_recv.at[j, c],
            device_id=at(sp, lax.rem(tp + j, n_tp)), device_id_type=MESH)

    def for_others(c):
        for j in range(1, n_tp):
            sums[j, c] = product(c, j).astype(jnp.bfloat16)
            sum_out(c, j).start()

    def for_self(c):
        total = product(c, 0).astype(jnp.bfloat16).astype(jnp.float32)
        for j in range(1, n_tp):
            sum_out(c, j).wait_recv()
            total += sums_in[j, c].astype(jnp.float32)
        mixed_ref[:, columns_of(c)] = total.astype(jnp.bfloat16)

    for c in range(chunks):
        if group == 4:
            for i in near:
                edge_in(nearest(c), i).wait_recv()
        for_others(c)
        if 0 < c < chunks - 1:
            for_self(c - 1)
    if chunks > 1:
        for_self(chunks - 2)
    for_self(chunks - 1)

    own_l.wait()
    for i in range(1, group):
        lse_in(i).wait_recv()
    for b in range(group):
        lse_out_ref[b * heads : (b + 1) * heads, :] = lse_all[b]

    for i in range(1, group):
        w_in_plane(i).wait_send()
        for k in range(2):
            for j in range(1, n_tp):
                across(i, k, j).wait_send()
    for i in near:
        for k in range(2):
            tokens_out(i, k).wait_send()
        if group == 4:
            corner_out(i).wait_send()
    if planes > 1:
        lax.fori_loop(1, planes, hops(relay_left), 0)
        lax.fori_loop(1, planes, lambda k, _: (o_relay_left(k), _)[1], 0)
    for h in range(1, far + 1):
        @pl.when(plane + h < planes)
        def _():
            for i in range(group):
                for k in range(2):
                    halo_out(h, i, k).wait_send()
    for j in range(1, n_tp):
        for c in range(chunks):
            sum_out(c, j).wait_send()
    for i in range(1, group):
        att_out(i).wait_send()
        lse_out(i).wait_send()
    if by_plane:
        for m in range(planes):
            for i in near:
                side_out(nearest(m), i).wait_send()
                if group == 4:
                    edge_out(nearest(m), i).wait_send()


def shards(n, n_tp, tokens, w_query, w_key, w_value, w_out):
    rows, model = tokens.shape
    depth, width = w_query.shape
    slabs = width // LANES
    reach = KEYS_BEHIND * dilation_rates[-1]
    group = 1
    while group < 4 and group * rows < reach and slabs % (2 * group) == 0 and n % (2 * group) == 0:
        group *= 2
    assert slabs == group
    far = (reach + group * rows - 1) // (group * rows)
    planes = n // group
    own = group * rows
    part = rows // n_tp
    heads = LANES // HEAD_SIZE

    turned = w_out.T
    cut = w_out.shape[1]
    behind = far * own
    chunks = planes if group > 1 else (4 if (n * cut) % (4 * LANES) == 0 else 1)
    chunk = n * cut // chunks

    f32, bf16 = jnp.float32, jnp.bfloat16
    dma = pltpu.SemaphoreType.DMA
    vmem = pl.BlockSpec(memory_space=VMEM)
    mixed, lse = pl.pallas_call(
        functools.partial(layer_kernel, n, n_tp, group, far, heads),
        out_shape=(
            jax.ShapeDtypeStruct((part, n * cut), bf16),
            jax.ShapeDtypeStruct((group * heads, rows), f32),
        ),
        in_specs=[pl.BlockSpec(memory_space=pltpu.HBM)] * 5,
        out_specs=(vmem, vmem),
        scratch_shapes=[
            VMEM((group, rows, model), bf16),
            VMEM((n, depth, 3 * LANES), bf16),
            VMEM((group, depth, 3 * LANES), bf16),
            VMEM((own, 2 * LANES), bf16), VMEM((far, own, 2 * LANES), bf16),
            VMEM((n * cut, width), bf16),
            VMEM((own, LANES), f32), VMEM((behind + own, LANES), f32), VMEM((behind + own, LANES), f32),
            VMEM((1 + len(dilation_rates), KEYS_BEHIND, 2 * KEYS_BEHIND), f32),
            VMEM((own, LANES), f32), VMEM((own, LANES), f32), VMEM((own, LANES), f32),
            VMEM((own, LANES), bf16), VMEM((group, heads, rows), f32), VMEM((group, heads, rows), f32),
            VMEM((group, rows, LANES), bf16),
            VMEM((n_tp, chunks, part, chunk), bf16), VMEM((n_tp, chunks, part, chunk), bf16),
            dma((3, group)), dma((4,)),
            dma((group,)), dma((group,)),
            dma((group, planes)), dma((group, planes)),
            dma((group, planes)), dma((group, planes)),
            dma((group, 2)), dma((group, 2)),
            dma((group,)), dma((group,)),
            dma((group, 2, n_tp)), dma((group, 2, n_tp)),
            dma((far + 1, group, 2)), dma((far + 1, group, 2)),
            dma((planes,)), dma((planes,)), dma((planes,)), dma((planes,)),
            dma((planes, group)), dma((planes, group)),
            dma((planes, group)), dma((planes, group)),
            dma((group,)), dma((group,)), dma((group,)), dma((group,)),
            dma((n_tp, chunks)), dma((n_tp, chunks)),
        ],
        compiler_params=pltpu.CompilerParams(collective_id=0, has_side_effects=True, vmem_limit_bytes=56 << 20),
        cost_estimate=pl.CostEstimate(
            flops=2 * own * model * 3 * LANES, bytes_accessed=1 << 24, transcendentals=1 << 22),
        name="layer",
    )(w_query, w_key, w_value, tokens, turned)
    return mixed, lse


def solution(mesh):
    placed = (P("sp", None), P("sp", "tp"), P("sp", "tp"), P("sp", "tp"), P("tp", "sp"))
    return jax.shard_map(
        functools.partial(shards, mesh.shape["sp"], mesh.shape["tp"]),
        mesh=mesh,
        in_specs=placed,
        out_specs=(P(("sp", "tp"), None), P("tp", "sp")),
        check_vma=False,
    )
```

time: 124 us -> 109 us (0.88)
  Pallas kernels: 118 us -> 105 us
  local copies, waits for them, and re-layouts: 5.46 us -> 3.27 us
    pallas_call x2 -> x1, Pallas kernels: 118 us -> 105 us  [shards(): pl.pallas_call(functools.partial(layer_kernel, n, n_tp, group, far, heads...]
    unnamed x9 -> x4, local copies, waits for them, and re-layouts: 4.84 us -> 3.27 us
where the time goes in v1:
time: 109 us
  Pallas kernels  105 us (96%)
  local copies, waits for them, and re-layouts  3.27 us (3%)
    pallas_call x1, Pallas kernels, shards(): pl.pallas_call(functools.partial(layer_kernel, n, n_tp, group, far, heads...  105 us
    unnamed x4, local copies, waits for them, and re-layouts  3.27 us

profile of v1, /device:TPU:0, one launch (start us, length us, event | category | flops | bytes accessed | tf_op | source)
XLA Modules:
  0.0 108.8 jit_solution(13381878137782051899)
XLA Ops:
  0.6 104.9 %layer.1 = (bf16[256,3072]{1,0:T(8,128)(2,1)}, f32[8,512]{1,0:T(8,128)}) custom-call(bf16[192,512]{1,0:T(8,128)(2,1)} %wq_ref.1, bf16[192,512]{1,0:T(8,128)(2,1)} %wk_ref.1, bf16[192,512]{1,0:T(8,128)(2,1)} %wv_ref.1, bf16[512,3072]{1,0:T(8,128)(2,1)} %tok_ref.1, bf16[192,512]{1,0:T(8,128)(2,1)} %bitcast.1), custom_call_target="tpu_custom_call" | custom-call | flops 4831838208 | bytes 16777216 | tf_op jit(solution)/shard_map/layer/pallas_call | solution.py:615
  105.5 0.0 copy-start
  105.5 2.7 %copy.9 = bf16[256,3072]{1,0:T(8,128)(2,1)} copy(bf16[256,3072]{1,0:T(8,128)(2,1)} %get-tuple-element.4) | data formatting | bytes 3145728
  108.2 0.0 copy-done
  108.2 0.6 copy.10
Async XLA Ops:
  105.5 2.7 %copy-start = (f32[8,512]{1,0:T(8,128)S(1)}, f32[8,512]{1,0:T(8,128)}, u32[]{:S(2)}) copy-start(f32[8,512]{1,0:T(8,128)} %get-tuple-element.5) | copy-start | bytes 49156

commit v2 on v1

--- a/solution.py
+++ b/solution.py
@@ -28,7 +28,7 @@
     att_all, sums, sums_in,
     pack_sem, own_sem, w1_send, w1_recv, up_send, up_recv, down_send, down_recv, t_send, t_recv, d_send, d_recv,
     f_send, f_recv, h_send, h_recv, ou_send, ou_recv, od_send, od_recv, b_send, b_recv, c_send, c_recv,
-    a_send, a_recv, l_send, l_recv, s_send, s_recv,
+    zu_send, zu_recv, zd_send, zd_recv, a_send, a_recv, l_send, l_recv, s_send, s_recv,
 ):
     sp, tp = lax.axis_index("sp"), lax.axis_index("tp")
     planes = n // group
@@ -160,6 +160,12 @@
 
         return one
 
+    def nearest(m):
+        left, right = plane, planes - 1 - plane
+        short = jnp.minimum(left, right)
+        zigzag = plane + (m // 2 if m % 2 == 0 else -((m + 1) // 2))
+        return jnp.where(m <= 2 * short, zigzag, jnp.where(left < right, m, planes - 1 - m))
+
     def back(q):
         return lax.rem(plane - q + planes, planes)
 
@@ -191,11 +197,47 @@
         for i in near:
             side_out(q, i).start()
 
-    def edges(q):
+    corner_hops = min(2, planes - 1) if group == 4 else 0
+
+    def edge_goes(m, action):
+        if group == 4:
+            if m == 0:
+                action()
+            elif m > corner_hops:
+                when(jnp.abs(nearest(m) - plane) > corner_hops, action)
+
+    def edges(m):
+        q = nearest(m)
         for i in near:
             side_in(q, i).wait_recv()
-            if group == 4:
-                edge_out(q, i).start()
+        edge_goes(m, lambda: [edge_out(q, i).start() for i in near])
+
+    def edges_arrive(m):
+        edge_goes(m, lambda: [edge_in(nearest(m), i).wait_recv() for i in near])
+
+    def z_up(k, p):
+        ref = strip(lax.rem(p + 2 * planes, planes), 3)
+        return pltpu.make_async_remote_copy(
+            src_ref=ref, dst_ref=ref, send_sem=zu_send.at[k], recv_sem=zu_recv.at[k],
+            device_id=at(above, tp), device_id_type=MESH)
+
+    def z_down(k, p):
+        ref = strip(lax.rem(p + 2 * planes, planes), 3)
+        return pltpu.make_async_remote_copy(
+            src_ref=ref, dst_ref=ref, send_sem=zd_send.at[k], recv_sem=zd_recv.at[k],
+            device_id=at(below, tp), device_id_type=MESH)
+
+    def z_relay(k):
+        when(~last & (plane - k + 1 >= 0), lambda: z_up(k, plane - k + 1).start())
+        when(~first & (plane + k - 1 < planes), lambda: z_down(k, plane + k - 1).start())
+
+    def z_relayed(k):
+        when(plane - k >= 0, lambda: z_up(k, plane - k).wait_recv())
+        when(plane + k < planes, lambda: z_down(k, plane + k).wait_recv())
+
+    def z_relay_left(k):
+        when(~last & (plane - k + 1 >= 0), lambda: z_up(k, plane - k + 1).wait_send())
+        when(~first & (plane + k - 1 < planes), lambda: z_down(k, plane + k - 1).wait_send())
 
     def o_relayed(k):
         def from_below():
@@ -215,6 +257,10 @@
     def unit(k, t):
         return pl.ds(pl.multiple_of(k * half + t * unit_rows, unit_rows), unit_rows)
 
+    def bit(k, t, s):
+        size = unit_rows // 2
+        return pl.ds(pl.multiple_of(k * half + t * unit_rows + s * size, size), size)
+
     def tokens_out(i, k):
         return pltpu.make_async_remote_copy(
             src_ref=tok_ref.at[unit(k, tp)], dst_ref=tok_all.at[g, unit(k, tp)],
@@ -225,33 +271,33 @@
             src_ref=tok_ref.at[unit(k, tp)], dst_ref=tok_all.at[g ^ i, unit(k, tp)],
             send_sem=t_send.at[i, k], recv_sem=t_recv.at[i, k], device_id=at(mate(i), tp), device_id_type=MESH)
 
-    def corner_out(i):
-        ref = tok_all.at[g ^ i, unit(i - 1, tp)]
-        return pltpu.make_async_remote_copy(
-            src_ref=ref, dst_ref=ref, send_sem=d_send.at[i], recv_sem=d_recv.at[i],
+    def corner_out(i, s):
+        ref = tok_all.at[g ^ i, bit(i - 1, tp, s)]
+        return pltpu.make_async_remote_copy(
+            src_ref=ref, dst_ref=ref, send_sem=d_send.at[i, s], recv_sem=d_recv.at[i, s],
             device_id=at(mate(3 - i), tp), device_id_type=MESH)
 
-    def corner_in(i):
-        ref = tok_all.at[g ^ 3, unit(i - 1, tp)]
-        return pltpu.make_async_remote_copy(
-            src_ref=ref, dst_ref=ref, send_sem=d_send.at[i], recv_sem=d_recv.at[i],
+    def corner_in(i, s):
+        ref = tok_all.at[g ^ 3, bit(i - 1, tp, s)]
+        return pltpu.make_async_remote_copy(
+            src_ref=ref, dst_ref=ref, send_sem=d_send.at[i, s], recv_sem=d_recv.at[i, s],
             device_id=at(mate(3 - i), tp), device_id_type=MESH)
 
-    def across(i, k, j):
-        ref = tok_all.at[g ^ i, unit(k, tp)]
-        return pltpu.make_async_remote_copy(
-            src_ref=ref, dst_ref=ref, send_sem=f_send.at[i, k, j], recv_sem=f_recv.at[i, k, j],
+    def across(i, k, s, j):
+        ref = tok_all.at[g ^ i, bit(k, tp, s)]
+        return pltpu.make_async_remote_copy(
+            src_ref=ref, dst_ref=ref, send_sem=f_send.at[i, k, s, j], recv_sem=f_recv.at[i, k, s, j],
             device_id=at(sp, lax.rem(tp + j, n_tp)), device_id_type=MESH)
 
-    def across_in(i, k, j):
-        ref = tok_all.at[g ^ i, unit(k, lax.rem(tp + n_tp - j, n_tp))]
-        return pltpu.make_async_remote_copy(
-            src_ref=ref, dst_ref=ref, send_sem=f_send.at[i, k, j], recv_sem=f_recv.at[i, k, j],
+    def across_in(i, k, s, j):
+        ref = tok_all.at[g ^ i, bit(k, lax.rem(tp + n_tp - j, n_tp), s)]
+        return pltpu.make_async_remote_copy(
+            src_ref=ref, dst_ref=ref, send_sem=f_send.at[i, k, s, j], recv_sem=f_recv.at[i, k, s, j],
             device_id=at(sp, lax.rem(tp + j, n_tp)), device_id_type=MESH)
 
-    def to_other_cores(i, k):
+    def to_other_cores(i, k, s):
         for j in range(1, n_tp):
-            across(i, k, j).start()
+            across(i, k, s, j).start()
 
     def piece(i, s):
         return s if i == 1 else 1 - s
@@ -296,15 +342,17 @@
         o_relay(1)
     for i in near:
         tokens_in(i, piece(i, 0)).wait_recv()
-        if group == 4:
-            corner_out(i).start()
-        to_other_cores(i, piece(i, 0))
+        for s in range(2):
+            if group == 4:
+                corner_out(i, s).start()
+            to_other_cores(i, piece(i, 0), s)
     if planes > 1:
         for i in range(group):
             relayed(planes - 1, i)
     for i in near:
         tokens_in(i, piece(i, 1)).wait_recv()
-        to_other_cores(i, piece(i, 1))
+        for s in range(2):
+            to_other_cores(i, piece(i, 1), s)
     if near:
         sides(plane)
     own_t.wait()
@@ -343,59 +391,37 @@
         lax.fori_loop(0, 2, one, 0)
 
     def crossed(i, k):
-        for j in range(1, n_tp):
-            across_in(i, k, j).wait_recv()
-
-    def o_step(k):
+        for s in range(2):
+            for j in range(1, n_tp):
+                across_in(i, k, s, j).wait_recv()
+
+    def o_pass(k):
         if k < planes:
             o_relayed(k)
-            o_sides(k)
             if k + 1 < planes:
                 o_relay(k + 1)
 
+    def o_spread(k):
+        if k < planes:
+            o_sides(k)
+
     tiles(lambda s: (0, s), lambda i, k: None)
     if group > 1:
-        o_step(1)
+        o_pass(1)
+        o_spread(1)
     if group == 2:
         tiles(lambda s: (1, s), crossed)
     if group == 4:
         tiles(lambda s: (1 + s, s), crossed)
-        o_step(2)
         tiles(lambda s: (1 + s, 1 - s), crossed)
-        o_step(3)
-        for k in (1, 2):
-            corner_in(k).wait_recv()
-            to_other_cores(3, k - 1)
+        o_pass(2)
+        for s in range(2):
+            for i in near:
+                corner_in(i, s).wait_recv()
+                to_other_cores(3, i - 1, s)
         tiles(lambda s: (3, s), crossed)
-    done = {1: 1, 2: 2, 4: 4}[group]
-
-    def o_rest(k, _):
-        o_relayed(k)
-        o_sides(k)
-        if True:
-            when(k + 1 < planes, lambda: o_relay(k + 1))
-        return _
-
-    if done < planes:
-        lax.fori_loop(done, planes, o_rest, 0)
-
-    def nearest(m):
-        left, right = plane, planes - 1 - plane
-        short = jnp.minimum(left, right)
-        zigzag = plane + (m // 2 if m % 2 == 0 else -((m + 1) // 2))
-        return jnp.where(m <= 2 * short, zigzag, jnp.where(left < right, m, planes - 1 - m))
 
     by_plane = group > 1
-    passed = 0
-
-    def edges_next():
-        nonlocal passed
-        if by_plane and passed < planes:
-            edges(nearest(passed))
-            passed += 1
-
-    low_of = {}
-
     def attention(number, begin, end, unroll):
         d = dilation_rates[number]
         step = min(KEYS_BEHIND, own // d)
@@ -443,10 +469,32 @@
     def unroll_of(trips):
         return next(u for u in (2, 3, 1) if trips % u == 0)
 
+    def later(k, _):
+        o_relayed(k)
+        when(k + 1 < planes, lambda: o_relay(k + 1))
+        o_sides(k)
+        return _
+
+    def before_second():
+        if by_plane:
+            edges(0)
+        if group == 4:
+            o_spread(2)
+        started = {1: 1, 2: 2, 4: 3}[group]
+        if started < planes:
+            lax.fori_loop(started, planes, later, 0)
+
+    def before_halo():
+        edges_arrive(0)
+        if corner_hops > 0:
+            z_relay(1)
+
     for number, d in enumerate(dilation_rates):
         if counts[number] > 1:
             attention(number, 1, counts[number], unroll_of((counts[number] - 1) * d))
-            edges_next()
+        if number == 0:
+            before_second()
+    before_halo()
 
     for h in range(1, far + 1):
         @pl.when(plane - h >= 0)
@@ -460,19 +508,24 @@
 
     for number, d in enumerate(dilation_rates):
         attention(number, 0, 1, unroll_of(d))
-        edges_next()
+    for k in range(1, corner_hops):
+        z_relayed(k)
+        z_relay(k + 1)
 
     att[...] = (acc_s[...] / den_s[...]).astype(jnp.bfloat16)
+
+    def att_lanes(i):
+        return att_all.at[:, pl.ds(pl.multiple_of((g ^ i) * LANES, LANES), LANES)]
 
     def att_out(i):
         mine = pl.ds(pl.multiple_of((g ^ i) * rows, rows), rows)
         return pltpu.make_async_remote_copy(
-            src_ref=att.at[mine], dst_ref=att_all.at[g], send_sem=a_send.at[i], recv_sem=a_recv.at[i],
+            src_ref=att.at[mine], dst_ref=att_lanes(0), send_sem=a_send.at[i], recv_sem=a_recv.at[i],
             device_id=at(mate(i), tp), device_id_type=MESH)
 
     def att_in(i):
         return pltpu.make_async_remote_copy(
-            src_ref=att.at[pl.ds(0, rows)], dst_ref=att_all.at[g ^ i], send_sem=a_send.at[i], recv_sem=a_recv.at[i],
+            src_ref=att.at[pl.ds(0, rows)], dst_ref=att_lanes(i), send_sem=a_send.at[i], recv_sem=a_recv.at[i],
             device_id=at(mate(i), tp), device_id_type=MESH)
 
     def lse_out(i):
@@ -487,8 +540,11 @@
 
     for i in range(1, group):
         att_out(i).start()
-    own_a = pltpu.make_async_copy(att.at[pl.ds(pl.multiple_of(g * rows, rows), rows)], att_all.at[g], own_sem.at[1])
+    own_a = pltpu.make_async_copy(att.at[pl.ds(pl.multiple_of(g * rows, rows), rows)], att_lanes(0), own_sem.at[1])
     own_a.start()
+    if by_plane:
+        for m in range(corner_hops + 1, planes):
+            edges(m)
 
     for t in range(own // LANES):
         at_rows = pl.ds(t * LANES, LANES)
@@ -501,53 +557,52 @@
     own_l = pltpu.make_async_copy(lse_ref.at[g], lse_all.at[g], own_sem.at[2])
     own_l.start()
 
-    while by_plane and passed < planes:
-        edges_next()
     own_a.wait()
     for i in range(1, group):
         att_in(i).wait_recv()
 
-    chunks, chunk = sums.shape[1], sums.shape[3]
+    chunks, chunk = sums.shape[0], sums.shape[2]
 
     def columns_of(m):
         if by_plane:
             return pl.ds(pl.multiple_of(nearest(m) * chunk, chunk), chunk)
         return pl.ds(m * chunk, chunk)
 
-    def product(c, j):
-        wanted = lax.rem(tp + j, n_tp)
-        here = pl.ds(pl.multiple_of(wanted * part, part), part)
-        a = jnp.concatenate([att_all[b, here, :] for b in range(group)], axis=1)
+    def rows_of(j):
+        return pl.ds(pl.multiple_of(lax.rem(tp + j, n_tp) * part, part), part)
+
+    def sum_out(c, j):
+        return pltpu.make_async_remote_copy(
+            src_ref=sums.at[c, rows_of(j)], dst_ref=sums_in.at[j, c], send_sem=s_send.at[j, c], recv_sem=s_recv.at[j, c],
+            device_id=at(sp, lax.rem(tp + j, n_tp)), device_id_type=MESH)
+
+    def multiply(c):
         w = o_all[columns_of(c), :]
-        return lax.dot_general(a, w, (((1,), (1,)), ((), ())), preferred_element_type=jnp.float32)
-
-    def sum_out(c, j):
-        return pltpu.make_async_remote_copy(
-            src_ref=sums.at[j, c], dst_ref=sums_in.at[j, c], send_sem=s_send.at[j, c], recv_sem=s_recv.at[j, c],
-            device_id=at(sp, lax.rem(tp + j, n_tp)), device_id_type=MESH)
-
-    def for_others(c):
+        product = lax.dot_general(att_all[...], w, (((1,), (1,)), ((), ())), preferred_element_type=jnp.float32)
+        sums[c] = product.astype(jnp.bfloat16)
         for j in range(1, n_tp):
-            sums[j, c] = product(c, j).astype(jnp.bfloat16)
             sum_out(c, j).start()
 
-    def for_self(c):
-        total = product(c, 0).astype(jnp.bfloat16).astype(jnp.float32)
+    def add_up(c):
+        total = sums[c, rows_of(0), :].astype(jnp.float32)
         for j in range(1, n_tp):
             sum_out(c, j).wait_recv()
             total += sums_in[j, c].astype(jnp.float32)
         mixed_ref[:, columns_of(c)] = total.astype(jnp.bfloat16)
 
     for c in range(chunks):
-        if group == 4:
-            for i in near:
-                edge_in(nearest(c), i).wait_recv()
-        for_others(c)
-        if 0 < c < chunks - 1:
-            for_self(c - 1)
-    if chunks > 1:
-        for_self(chunks - 2)
-    for_self(chunks - 1)
+        if by_plane:
+            if 0 < c <= corner_hops:
+                for i in near:
+                    side_in(nearest(c), i).wait_recv()
+            if c == 1 and corner_hops > 0:
+                z_relayed(corner_hops)
+            if c > 0:
+                edges_arrive(c)
+        multiply(c)
+        if c > 0:
+            add_up(c - 1)
+    add_up(chunks - 1)
 
     own_l.wait()
     for i in range(1, group):
@@ -558,13 +613,14 @@
     for i in range(1, group):
         w_in_plane(i).wait_send()
         for k in range(2):
-            for j in range(1, n_tp):
-                across(i, k, j).wait_send()
+            for s in range(2):
+                for j in range(1, n_tp):
+                    across(i, k, s, j).wait_send()
     for i in near:
         for k in range(2):
             tokens_out(i, k).wait_send()
-        if group == 4:
-            corner_out(i).wait_send()
+            if group == 4:
+                corner_out(i, k).wait_send()
     if planes > 1:
         lax.fori_loop(1, planes, hops(relay_left), 0)
         lax.fori_loop(1, planes, lambda k, _: (o_relay_left(k), _)[1], 0)
@@ -584,8 +640,9 @@
         for m in range(planes):
             for i in near:
                 side_out(nearest(m), i).wait_send()
-                if group == 4:
-                    edge_out(nearest(m), i).wait_send()
+            edge_goes(m, lambda m=m: [edge_out(nearest(m), i).wait_send() for i in near])
+        for k in range(1, corner_hops + 1):
+            z_relay_left(k)
 
 
 def shards(n, n_tp, tokens, w_query, w_key, w_value, w_out):
@@ -630,23 +687,24 @@
             VMEM((1 + len(dilation_rates), KEYS_BEHIND, 2 * KEYS_BEHIND), f32),
             VMEM((own, LANES), f32), VMEM((own, LANES), f32), VMEM((own, LANES), f32),
             VMEM((own, LANES), bf16), VMEM((group, heads, rows), f32), VMEM((group, heads, rows), f32),
-            VMEM((group, rows, LANES), bf16),
-            VMEM((n_tp, chunks, part, chunk), bf16), VMEM((n_tp, chunks, part, chunk), bf16),
+            VMEM((rows, group * LANES), bf16),
+            VMEM((chunks, rows, chunk), bf16), VMEM((n_tp, chunks, part, chunk), bf16),
             dma((3, group)), dma((4,)),
             dma((group,)), dma((group,)),
             dma((group, planes)), dma((group, planes)),
             dma((group, planes)), dma((group, planes)),
             dma((group, 2)), dma((group, 2)),
-            dma((group,)), dma((group,)),
-            dma((group, 2, n_tp)), dma((group, 2, n_tp)),
+            dma((group, 2)), dma((group, 2)),
+            dma((group, 2, 2, n_tp)), dma((group, 2, 2, n_tp)),
             dma((far + 1, group, 2)), dma((far + 1, group, 2)),
             dma((planes,)), dma((planes,)), dma((planes,)), dma((planes,)),
             dma((planes, group)), dma((planes, group)),
             dma((planes, group)), dma((planes, group)),
+            dma((3,)), dma((3,)), dma((3,)), dma((3,)),
             dma((group,)), dma((group,)), dma((group,)), dma((group,)),
             dma((n_tp, chunks)), dma((n_tp, chunks)),
         ],
-        compiler_params=pltpu.CompilerParams(collective_id=0, has_side_effects=True, vmem_limit_bytes=56 << 20),
+        compiler_params=pltpu.CompilerParams(collective_id=0, has_side_effects=True, vmem_limit_bytes=46 << 20),
         cost_estimate=pl.CostEstimate(
             flops=2 * own * model * 3 * LANES, bytes_accessed=1 << 24, transcendentals=1 << 22),
         name="layer",

time: 109 us -> 109 us (level)
  Pallas kernels: 105 us -> 100 us
  local copies, waits for them, and re-layouts: 3.27 us -> 7.34 us
    pallas_call x1, Pallas kernels: 105 us -> 100 us  [shards(): pl.pallas_call(functools.partial(layer_kernel, n, n_tp, group, far, heads...]
    unnamed x4 -> x12, local copies, waits for them, and re-layouts: 3.27 us -> 7.34 us
where the time goes in v2:
time: 109 us; the launch traced here: 108 us
  Pallas kernels  100 us (92%)
  local copies, waits for them, and re-layouts  7.34 us (7%)
    pallas_call x1, Pallas kernels, shards(): pl.pallas_call(functools.partial(layer_kernel, n, n_tp, group, far, heads...  100 us
    unnamed x12, local copies, waits for them, and re-layouts  7.34 us

profile of v2, /device:TPU:0, one launch (start us, length us, event | category | flops | bytes accessed | tf_op | source)
XLA Modules:
  0.0 108.4 jit_solution(14342798331188886561)
XLA Ops:
  0.6 0.0 copy-start
  0.6 1.9 %copy-done = bf16[512,3072]{1,0:T(8,128)(2,1)S(1)} copy-done((bf16[512,3072]{1,0:T(8,128)(2,1)S(1)}, bf16[512,3072]{1,0:T(8,128)(2,1)}, u32[]{:S(2)}) %copy-start) | copy-done | bytes 3145752
  2.5 0.0 copy-start.1
  2.5 0.9 copy-done.1
  3.4 0.0 copy-start.2
  3.5 0.9 copy-done.2
  4.4 0.0 copy-start.3
  4.4 0.9 copy-done.3
  5.3 0.0 copy-start.4
  5.3 0.9 copy-done.4
  6.2 100.4 %layer.1 = (bf16[256,3072]{1,0:T(8,128)(2,1)S(1)}, f32[8,512]{1,0:T(8,128)S(1)}) custom-call(bf16[192,512]{1,0:T(8,128)(2,1)S(1)} %copy-done.1, bf16[192,512]{1,0:T(8,128)(2,1)S(1)} %copy-done.2, bf16[192,512]{1,0:T(8,128)(2,1)S(1)} %copy-done.3, bf16[512,3072]{1,0:T(8,128)(2,1)S(1)} %copy-done, bf16[192,512]{1,0:T(8,128)(2,1)S(1)} %bitcast.1), custom_call_target="tpu_custom_call" | custom-call | flops 4831838208 | bytes 16777216 | tf_op jit(solution)/shard_map/layer/pallas_call | solution.py:672
  106.6 1.1 %copy.9 = bf16[256,3072]{1,0:T(8,128)(2,1)} copy(bf16[256,3072]{1,0:T(8,128)(2,1)S(1)} %get-tuple-element.4) | data formatting | bytes 3145728
  107.8 0.6 copy.10
Async XLA Ops:
  0.6 1.9 %copy-start = (bf16[512,3072]{1,0:T(8,128)(2,1)S(1)}, bf16[512,3072]{1,0:T(8,128)(2,1)}, u32[]{:S(2)}) copy-start(bf16[512,3072]{1,0:T(8,128)(2,1)} %tok_ref.1) | copy-start | bytes 9437188
  2.5 0.9 copy-start.1
  3.4 0.9 copy-start.2
  4.4 0.9 copy-start.3
  5.3 0.9 copy-start.4

commit v3 on v2

--- a/solution.py
+++ b/solution.py
@@ -37,7 +37,7 @@
     own = group * rows
     base = plane * own
     half = rows // 2
-    unit_rows = half // n_tp
+    bit_rows = half // (2 * n_tp)
     part = mixed_ref.shape[0]
     cut, width = o_ref.shape
     half_cut = cut // 2
@@ -193,9 +193,9 @@
             src_ref=strip(q, 3, i - 1), dst_ref=strip(q, 3, i - 1), send_sem=c_send.at[k, i], recv_sem=c_recv.at[k, i],
             device_id=at(mate(3 - i), tp), device_id_type=MESH)
 
-    def sides(q):
+    def sides(m):
         for i in near:
-            side_out(q, i).start()
+            side_out(nearest(m), i).start()
 
     corner_hops = min(2, planes - 1) if group == 4 else 0
 
@@ -207,10 +207,9 @@
                 when(jnp.abs(nearest(m) - plane) > corner_hops, action)
 
     def edges(m):
-        q = nearest(m)
         for i in near:
-            side_in(q, i).wait_recv()
-        edge_goes(m, lambda: [edge_out(q, i).start() for i in near])
+            side_in(nearest(m), i).wait_recv()
+        edge_goes(m, lambda: [edge_out(nearest(m), i).start() for i in near])
 
     def edges_arrive(m):
         edge_goes(m, lambda: [edge_in(nearest(m), i).wait_recv() for i in near])
@@ -231,9 +230,22 @@
         when(~last & (plane - k + 1 >= 0), lambda: z_up(k, plane - k + 1).start())
         when(~first & (plane + k - 1 < planes), lambda: z_down(k, plane + k - 1).start())
 
+    def z_forward(k):
+        def up_on():
+            z_up(k, plane - k).wait_recv()
+            z_up(k + 1, plane - k).start()
+
+        def down_on():
+            z_down(k, plane + k).wait_recv()
+            z_down(k + 1, plane + k).start()
+
+        when(~last & (plane - k >= 0), up_on)
+        when(~first & (plane + k < planes), down_on)
+
     def z_relayed(k):
-        when(plane - k >= 0, lambda: z_up(k, plane - k).wait_recv())
-        when(plane + k < planes, lambda: z_down(k, plane + k).wait_recv())
+        ends = (True, True) if k == corner_hops else (last, first)
+        when(ends[0] & (plane - k >= 0), lambda: z_up(k, plane - k).wait_recv())
+        when(ends[1] & (plane + k < planes), lambda: z_down(k, plane + k).wait_recv())
 
     def z_relay_left(k):
         when(~last & (plane - k + 1 >= 0), lambda: z_up(k, plane - k + 1).wait_send())
@@ -249,58 +261,49 @@
         when(plane - k >= 0, from_below)
         when(plane + k < planes, from_above)
 
-    def o_sides(k):
-        if near:
-            when(plane - k >= 0, lambda: sides(plane - k))
-            when(plane + k < planes, lambda: sides(plane + k))
-
-    def unit(k, t):
-        return pl.ds(pl.multiple_of(k * half + t * unit_rows, unit_rows), unit_rows)
-
-    def bit(k, t, s):
-        size = unit_rows // 2
-        return pl.ds(pl.multiple_of(k * half + t * unit_rows + s * size, size), size)
-
-    def tokens_out(i, k):
-        return pltpu.make_async_remote_copy(
-            src_ref=tok_ref.at[unit(k, tp)], dst_ref=tok_all.at[g, unit(k, tp)],
-            send_sem=t_send.at[i, k], recv_sem=t_recv.at[i, k], device_id=at(mate(i), tp), device_id_type=MESH)
-
-    def tokens_in(i, k):
-        return pltpu.make_async_remote_copy(
-            src_ref=tok_ref.at[unit(k, tp)], dst_ref=tok_all.at[g ^ i, unit(k, tp)],
-            send_sem=t_send.at[i, k], recv_sem=t_recv.at[i, k], device_id=at(mate(i), tp), device_id_type=MESH)
+    def bit(s, p, t):
+        return pl.ds(pl.multiple_of(s * half + (p * n_tp + t) * bit_rows, bit_rows), bit_rows)
+
+    def tokens_out(i, p, s):
+        return pltpu.make_async_remote_copy(
+            src_ref=tok_ref.at[bit(s, p, tp)], dst_ref=tok_all.at[g, bit(s, p, tp)],
+            send_sem=t_send.at[i, p, s], recv_sem=t_recv.at[i, p, s], device_id=at(mate(i), tp), device_id_type=MESH)
+
+    def tokens_in(i, p, s):
+        return pltpu.make_async_remote_copy(
+            src_ref=tok_ref.at[bit(s, p, tp)], dst_ref=tok_all.at[g ^ i, bit(s, p, tp)],
+            send_sem=t_send.at[i, p, s], recv_sem=t_recv.at[i, p, s], device_id=at(mate(i), tp), device_id_type=MESH)
 
     def corner_out(i, s):
-        ref = tok_all.at[g ^ i, bit(i - 1, tp, s)]
+        ref = tok_all.at[g ^ i, bit(s, i - 1, tp)]
         return pltpu.make_async_remote_copy(
             src_ref=ref, dst_ref=ref, send_sem=d_send.at[i, s], recv_sem=d_recv.at[i, s],
             device_id=at(mate(3 - i), tp), device_id_type=MESH)
 
     def corner_in(i, s):
-        ref = tok_all.at[g ^ 3, bit(i - 1, tp, s)]
+        ref = tok_all.at[g ^ 3, bit(s, i - 1, tp)]
         return pltpu.make_async_remote_copy(
             src_ref=ref, dst_ref=ref, send_sem=d_send.at[i, s], recv_sem=d_recv.at[i, s],
             device_id=at(mate(3 - i), tp), device_id_type=MESH)
 
-    def across(i, k, s, j):
-        ref = tok_all.at[g ^ i, bit(k, tp, s)]
-        return pltpu.make_async_remote_copy(
-            src_ref=ref, dst_ref=ref, send_sem=f_send.at[i, k, s, j], recv_sem=f_recv.at[i, k, s, j],
+    def across(i, p, s, j):
+        ref = tok_all.at[g ^ i, bit(s, p, tp)]
+        return pltpu.make_async_remote_copy(
+            src_ref=ref, dst_ref=ref, send_sem=f_send.at[i, p, s, j], recv_sem=f_recv.at[i, p, s, j],
             device_id=at(sp, lax.rem(tp + j, n_tp)), device_id_type=MESH)
 
-    def across_in(i, k, s, j):
-        ref = tok_all.at[g ^ i, bit(k, lax.rem(tp + n_tp - j, n_tp), s)]
-        return pltpu.make_async_remote_copy(
-            src_ref=ref, dst_ref=ref, send_sem=f_send.at[i, k, s, j], recv_sem=f_recv.at[i, k, s, j],
+    def across_in(i, p, s, j):
+        ref = tok_all.at[g ^ i, bit(s, p, lax.rem(tp + n_tp - j, n_tp))]
+        return pltpu.make_async_remote_copy(
+            src_ref=ref, dst_ref=ref, send_sem=f_send.at[i, p, s, j], recv_sem=f_recv.at[i, p, s, j],
             device_id=at(sp, lax.rem(tp + j, n_tp)), device_id_type=MESH)
 
-    def to_other_cores(i, k, s):
+    def to_other_cores(i, p, s):
         for j in range(1, n_tp):
-            across(i, k, s, j).start()
-
-    def piece(i, s):
-        return s if i == 1 else 1 - s
+            across(i, p, s, j).start()
+
+    def piece(i, step):
+        return step if i == 1 else 1 - step
 
     for i in range(1, group):
         for t in range(3):
@@ -310,9 +313,10 @@
         pack(t, 0).wait()
     if planes > 1:
         relay(1, 0)
-    for s in range(2):
-        for i in near:
-            tokens_out(i, piece(i, s)).start()
+    for step in range(2):
+        for s in range(2):
+            for i in near:
+                tokens_out(i, piece(i, step), s).start()
     for i in range(1, group):
         w_in_plane_arrives(i).wait_recv()
         if planes > 1:
@@ -340,21 +344,21 @@
     own_o.wait()
     if planes > 1:
         o_relay(1)
-    for i in near:
-        tokens_in(i, piece(i, 0)).wait_recv()
-        for s in range(2):
+    for s in range(2):
+        for i in near:
+            tokens_in(i, piece(i, 0), s).wait_recv()
             if group == 4:
                 corner_out(i, s).start()
             to_other_cores(i, piece(i, 0), s)
     if planes > 1:
         for i in range(group):
             relayed(planes - 1, i)
-    for i in near:
-        tokens_in(i, piece(i, 1)).wait_recv()
-        for s in range(2):
+    for s in range(2):
+        for i in near:
+            tokens_in(i, piece(i, 1), s).wait_recv()
             to_other_cores(i, piece(i, 1), s)
     if near:
-        sides(plane)
+        sides(0)
     own_t.wait()
 
     def halo_out(h, i, k):
@@ -391,9 +395,9 @@
         lax.fori_loop(0, 2, one, 0)
 
     def crossed(i, k):
-        for s in range(2):
+        for p in range(2):
             for j in range(1, n_tp):
-                across_in(i, k, s, j).wait_recv()
+                across_in(i, p, k, j).wait_recv()
 
     def o_pass(k):
         if k < planes:
@@ -401,25 +405,22 @@
             if k + 1 < planes:
                 o_relay(k + 1)
 
-    def o_spread(k):
-        if k < planes:
-            o_sides(k)
-
     tiles(lambda s: (0, s), lambda i, k: None)
     if group > 1:
         o_pass(1)
-        o_spread(1)
     if group == 2:
         tiles(lambda s: (1, s), crossed)
     if group == 4:
-        tiles(lambda s: (1 + s, s), crossed)
-        tiles(lambda s: (1 + s, 1 - s), crossed)
-        o_pass(2)
+        tiles(lambda s: (1 + s, 0), crossed)
+        tiles(lambda s: (1 + s, 1), crossed)
         for s in range(2):
             for i in near:
                 corner_in(i, s).wait_recv()
                 to_other_cores(3, i - 1, s)
-        tiles(lambda s: (3, s), crossed)
+            crossed(3, s)
+            tile(3, s)
+            if s == 0:
+                o_pass(2)
 
     by_plane = group > 1
     def attention(number, begin, end, unroll):
@@ -469,22 +470,29 @@
     def unroll_of(trips):
         return next(u for u in (2, 3, 1) if trips % u == 0)
 
+    strips = list(range(planes)) if by_plane else []
+    if 0 < corner_hops < planes - 1:
+        strips.remove(corner_hops)
+        strips.append(corner_hops)
+    early, late = strips[1:3], strips[3:]
+
     def later(k, _):
         o_relayed(k)
         when(k + 1 < planes, lambda: o_relay(k + 1))
-        o_sides(k)
         return _
 
     def before_second():
         if by_plane:
             edges(0)
-        if group == 4:
-            o_spread(2)
+            for m in early[:1]:
+                sides(m)
+
+    def before_halo():
         started = {1: 1, 2: 2, 4: 3}[group]
         if started < planes:
             lax.fori_loop(started, planes, later, 0)
-
-    def before_halo():
+        for m in early[1:]:
+            sides(m)
         edges_arrive(0)
         if corner_hops > 0:
             z_relay(1)
@@ -507,10 +515,12 @@
             vs[to] = halo_ref[far - h, :, LANES:].astype(jnp.float32)
 
     for number, d in enumerate(dilation_rates):
+        if number == 2:
+            for m in late:
+                sides(m)
         attention(number, 0, 1, unroll_of(d))
     for k in range(1, corner_hops):
-        z_relayed(k)
-        z_relay(k + 1)
+        z_forward(k)
 
     att[...] = (acc_s[...] / den_s[...]).astype(jnp.bfloat16)
 
@@ -542,9 +552,8 @@
         att_out(i).start()
     own_a = pltpu.make_async_copy(att.at[pl.ds(pl.multiple_of(g * rows, rows), rows)], att_lanes(0), own_sem.at[1])
     own_a.start()
-    if by_plane:
-        for m in range(corner_hops + 1, planes):
-            edges(m)
+    for m in early:
+        edges(m)
 
     for t in range(own // LANES):
         at_rows = pl.ds(t * LANES, LANES)
@@ -563,10 +572,14 @@
 
     chunks, chunk = sums.shape[0], sums.shape[2]
 
-    def columns_of(m):
+    per_strip = chunks // planes if by_plane else 1
+
+    def columns_of(c):
         if by_plane:
-            return pl.ds(pl.multiple_of(nearest(m) * chunk, chunk), chunk)
-        return pl.ds(m * chunk, chunk)
+            m, side = strips[c // per_strip], c % per_strip
+            side = side ^ (g // (group // per_strip)) if per_strip > 1 else 0
+            return pl.ds(pl.multiple_of((nearest(m) * per_strip + side) * chunk, chunk), chunk)
+        return pl.ds(c * chunk, chunk)
 
     def rows_of(j):
         return pl.ds(pl.multiple_of(lax.rem(tp + j, n_tp) * part, part), part)
@@ -590,15 +603,22 @@
             total += sums_in[j, c].astype(jnp.float32)
         mixed_ref[:, columns_of(c)] = total.astype(jnp.bfloat16)
 
+    def edges_arrive_late(m):
+        if m > 0:
+            edges_arrive(m)
+        if m == 1 and corner_hops > 0:
+            z_relayed(1)
+        if m > 1 and m == strips[2] and corner_hops > 1:
+            z_relayed(2)
+
     for c in range(chunks):
         if by_plane:
-            if 0 < c <= corner_hops:
-                for i in near:
-                    side_in(nearest(c), i).wait_recv()
-            if c == 1 and corner_hops > 0:
-                z_relayed(corner_hops)
-            if c > 0:
-                edges_arrive(c)
+            m, side = strips[c // per_strip], c % per_strip
+            if side == 0:
+                if m in late:
+                    edges(m)
+            if side == per_strip - 1:
+                edges_arrive_late(m)
         multiply(c)
         if c > 0:
             add_up(c - 1)
@@ -617,10 +637,11 @@
                 for j in range(1, n_tp):
                     across(i, k, s, j).wait_send()
     for i in near:
-        for k in range(2):
-            tokens_out(i, k).wait_send()
+        for s in range(2):
+            for p in range(2):
+                tokens_out(i, p, s).wait_send()
             if group == 4:
-                corner_out(i, k).wait_send()
+                corner_out(i, s).wait_send()
     if planes > 1:
         lax.fori_loop(1, planes, hops(relay_left), 0)
         lax.fori_loop(1, planes, lambda k, _: (o_relay_left(k), _)[1], 0)
@@ -663,7 +684,7 @@
     turned = w_out.T
     cut = w_out.shape[1]
     behind = far * own
-    chunks = planes if group > 1 else (4 if (n * cut) % (4 * LANES) == 0 else 1)
+    chunks = planes * (2 if group == 4 and 2 * cut % LANES == 0 else 1) if group > 1 else (4 if (n * cut) % (4 * LANES) == 0 else 1)
     chunk = n * cut // chunks
 
     f32, bf16 = jnp.float32, jnp.bfloat16
@@ -693,7 +714,7 @@
             dma((group,)), dma((group,)),
             dma((group, planes)), dma((group, planes)),
             dma((group, planes)), dma((group, planes)),
-            dma((group, 2)), dma((group, 2)),
+            dma((group, 2, 2)), dma((group, 2, 2)),
             dma((group, 2)), dma((group, 2)),
             dma((group, 2, 2, n_tp)), dma((group, 2, 2, n_tp)),
             dma((far + 1, group, 2)), dma((far + 1, group, 2)),
@@ -708,7 +729,7 @@
         cost_estimate=pl.CostEstimate(
             flops=2 * own * model * 3 * LANES, bytes_accessed=1 << 24, transcendentals=1 << 22),
         name="layer",
-    )(w_query, w_key, w_value, tokens, turned)
+    )(*[pltpu.with_memory_space_constraint(x, pltpu.HBM) for x in (w_query, w_key, w_value, tokens, turned)])
     return mixed, lse
 
 

time: 109 us -> 106 us (0.972)
  local copies, waits for them, and re-layouts: 7.34 us -> 1.75 us
  Pallas kernels: 100 us -> 104 us
    unnamed x12 -> x2, local copies, waits for them, and re-layouts: 7.34 us -> 1.75 us
    pallas_call x1, Pallas kernels: 100 us -> 104 us  [shards(): pl.pallas_call(functools.partial(layer_kernel, n, n_tp, group, far, heads...]
where the time goes in v3:
time: 106 us
  Pallas kernels  104 us (98%)
  local copies, waits for them, and re-layouts  1.75 us (2%)
    pallas_call x1, Pallas kernels, shards(): pl.pallas_call(functools.partial(layer_kernel, n, n_tp, group, far, heads...  104 us

profile of v3, /device:TPU:0, one launch (start us, length us, event | category | flops | bytes accessed | tf_op | source)
XLA Modules:
  0.0 105.9 jit_solution(8749448938369264039)
XLA Ops:
  0.6 103.5 %layer.1 = (bf16[256,3072]{1,0:T(8,128)(2,1)S(1)}, f32[8,512]{1,0:T(8,128)S(1)}) custom-call(bf16[192,512]{1,0:T(8,128)(2,1)} %wq_ref.1, bf16[192,512]{1,0:T(8,128)(2,1)} %wk_ref.1, bf16[192,512]{1,0:T(8,128)(2,1)} %wv_ref.1, bf16[512,3072]{1,0:T(8,128)(2,1)} %tok_ref.1, bf16[192,512]{1,0:T(8,128)(2,1)} %bitcast.1), custom_call_target="tpu_custom_call" | custom-call | flops 4831838208 | bytes 16777216 | tf_op jit(solution)/shard_map/layer/pallas_call | solution.py:693
  104.1 1.1 %copy.9 = bf16[256,3072]{1,0:T(8,128)(2,1)} copy(bf16[256,3072]{1,0:T(8,128)(2,1)S(1)} %get-tuple-element.4) | data formatting | bytes 3145728
  105.3 0.6 copy.10

commit v4 on v3

--- a/solution.py
+++ b/solution.py
@@ -24,8 +24,8 @@
 
 def layer_kernel(
     n, n_tp, group, far, heads, wq_ref, wk_ref, wv_ref, tok_ref, o_ref, mixed_ref, lse_out_ref,
-    tok_all, w_all, w_ref, kv_ref, halo_ref, o_all, qs, ks, vs, bias, top_s, den_s, acc_s, att, lse_ref, lse_all,
-    att_all, sums, sums_in,
+    tok_all, w_all, w_ref, kv_ref, halo_ref, o_all, qs, ks, vs, q_cls, k_cls, v_cls, out_cls, lse_cls, turn, bias,
+    top_s, den_s, acc_s, att, lse_ref, lse_all, att_all, sums, sums_in,
     pack_sem, own_sem, w1_send, w1_recv, up_send, up_recv, down_send, down_recv, t_send, t_recv, d_send, d_recv,
     f_send, f_recv, h_send, h_recv, ou_send, ou_recv, od_send, od_recv, b_send, b_recv, c_send, c_recv,
     zu_send, zu_recv, zd_send, zd_recv, a_send, a_recv, l_send, l_recv, s_send, s_recv,
@@ -41,7 +41,10 @@
     part = mixed_ref.shape[0]
     cut, width = o_ref.shape
     half_cut = cut // 2
-    behind = far * own
+    wide = dilation_rates[-1]
+    behind = KEYS_BEHIND * dilation_rates[-2]
+    run = half // wide
+    old = far * own // wide
 
     above = lax.rem(sp + group, n)
     below = lax.rem(sp + n - group, n)
@@ -333,11 +336,22 @@
     bias[0] = jnp.where(band, 0.0, neg_big)
     for number, d in enumerate(dilation_rates):
         bias[1 + number] = jnp.where(band & (base // d - KEYS_BEHIND + col >= 0), 0.0, neg_big)
+    to_row = lax.broadcasted_iota(jnp.int32, (half, half), 0)
+    from_row = lax.broadcasted_iota(jnp.int32, (half, half), 1)
+    turn[0] = (from_row == to_row % run * wide + to_row // run).astype(jnp.float32).astype(jnp.bfloat16)
+    turn[1] = (from_row == to_row % wide * run + to_row // wide).astype(jnp.float32).astype(jnp.bfloat16)
+
+    @pl.when(plane == 0)
+    def _():
+        ks[:behind] = jnp.zeros((behind, LANES), jnp.float32)
+        vs[:behind] = jnp.zeros((behind, LANES), jnp.float32)
+
     for h in range(1, far + 1):
         @pl.when(plane - h < 0)
         def _():
-            ks[(far - h) * own : (far - h + 1) * own] = jnp.zeros((own, LANES), jnp.float32)
-            vs[(far - h) * own : (far - h + 1) * own] = jnp.zeros((own, LANES), jnp.float32)
+            gone = slice((far - h) * own // wide, (far - h + 1) * own // wide)
+            k_cls[:, gone] = jnp.zeros((wide, own // wide, LANES), jnp.bfloat16)
+            v_cls[:, gone] = jnp.zeros((wide, own // wide, LANES), jnp.bfloat16)
 
     if planes > 1:
         lax.fori_loop(1, planes - 1, hops(pass_on), 0)
@@ -368,6 +382,10 @@
             send_sem=h_send.at[h, i, k], recv_sem=h_recv.at[h, i, k],
             device_id=at(lax.rem(sp + h * group, n), tp), device_id_type=MESH)
 
+    def by_classes(y):
+        sorted_rows = jnp.dot(turn[0], y, preferred_element_type=jnp.float32).astype(jnp.bfloat16)
+        return sorted_rows.reshape(wide, run, y.shape[1])
+
     def tile(i, k):
         block = g ^ i
         x = tok_all[block, pl.ds(pl.multiple_of(k * half, half), half), :]
@@ -380,6 +398,12 @@
         qs[to, :] = y[:, :LANES].astype(jnp.float32) * HEAD_SIZE ** (-0.5)
         ks[past, :] = y[:, LANES : 2 * LANES].astype(jnp.float32)
         vs[past, :] = y[:, 2 * LANES :].astype(jnp.float32)
+        by_class = by_classes(y)
+        at_run = pl.ds(pl.multiple_of(start // wide, run), run)
+        q_cls[:, at_run, :] = by_class[:, :, :LANES] * HEAD_SIZE ** (-0.5)
+        past_run = pl.ds(pl.multiple_of(old + start // wide, run), run)
+        k_cls[:, past_run, :] = by_class[:, :, LANES : 2 * LANES]
+        v_cls[:, past_run, :] = by_class[:, :, 2 * LANES :]
         for h in range(1, far + 1):
             @pl.when(plane + h < planes)
             def _():
@@ -465,7 +489,28 @@
 
         lax.fori_loop(begin * d, end * d, block, 0, unroll=unroll)
 
-    counts = [own // d // min(KEYS_BEHIND, own // d) for d in dilation_rates]
+    def wide_attention(cls, _):
+        step = own // wide
+        span = step + KEYS_BEHIND
+        q = q_cls[cls].astype(jnp.float32)
+        k = k_cls[cls, old - KEYS_BEHIND :, :]
+        v = v_cls[cls, old - KEYS_BEHIND :, :]
+        v = jnp.concatenate([v, jnp.ones((span, LANES), jnp.bfloat16)], axis=1)
+        low = lax.broadcasted_iota(jnp.int32, (step, LANES), 1) < HEAD_SIZE
+        q2 = jnp.concatenate([jnp.where(low, q, 0.0), jnp.where(low, 0.0, q)], axis=0).astype(jnp.bfloat16)
+        s = lax.dot_general(q2, k, (((1,), (1,)), ((), ())), preferred_element_type=jnp.float32)
+        seen = bias[len(dilation_rates), :step, :span]
+        s = s + jnp.concatenate([seen, seen], axis=0)
+        top = jnp.max(s, axis=1, keepdims=True)
+        p = jnp.exp(s - top)
+        o = jnp.dot(p.astype(jnp.bfloat16), v, preferred_element_type=jnp.float32)
+        top = jnp.where(low, top[:step], top[step:])
+        den = jnp.where(low, o[:step, LANES:], o[step:, LANES:])
+        out_cls[cls] = jnp.where(low, o[:step, :LANES], o[step:, :LANES]) / den
+        lse_cls[cls] = top + jnp.log(den)
+        return _
+
+    counts = [own // d // min(KEYS_BEHIND, own // d) for d in dilation_rates[:-1]]
 
     def unroll_of(trips):
         return next(u for u in (2, 3, 1) if trips % u == 0)
@@ -497,7 +542,7 @@
         if corner_hops > 0:
             z_relay(1)
 
-    for number, d in enumerate(dilation_rates):
+    for number, d in enumerate(dilation_rates[:-1]):
         if counts[number] > 1:
             attention(number, 1, counts[number], unroll_of((counts[number] - 1) * d))
         if number == 0:
@@ -507,23 +552,27 @@
     for h in range(1, far + 1):
         @pl.when(plane - h >= 0)
         def _():
-            for i in range(group):
-                for k in range(2):
-                    halo_out(h, i, k).wait_recv()
-            to = slice((far - h) * own, (far - h + 1) * own)
-            ks[to] = halo_ref[far - h, :, :LANES].astype(jnp.float32)
-            vs[to] = halo_ref[far - h, :, LANES:].astype(jnp.float32)
-
-    for number, d in enumerate(dilation_rates):
-        if number == 2:
-            for m in late:
-                sides(m)
+            def sort(u, _):
+                i, k = u // 2, lax.rem(u, 2)
+                halo_out(h, i, k).wait_recv()
+                start = (g ^ i) * rows + k * half
+                by_class = by_classes(halo_ref[far - h, pl.ds(pl.multiple_of(start, half), half), :])
+                at_run = pl.ds(pl.multiple_of((far - h) * (own // wide) + start // wide, run), run)
+                k_cls[:, at_run, :] = by_class[:, :, :LANES]
+                v_cls[:, at_run, :] = by_class[:, :, LANES:]
+                return _
+
+            lax.fori_loop(0, 2 * group, sort, 0)
+            if h == 1:
+                ks[:behind] = halo_ref[far - 1, own - behind :, :LANES].astype(jnp.float32)
+                vs[:behind] = halo_ref[far - 1, own - behind :, LANES:].astype(jnp.float32)
+
+    for number, d in enumerate(dilation_rates[:-1]):
         attention(number, 0, 1, unroll_of(d))
+    lax.fori_loop(0, wide, wide_attention, 0, unroll=2)
     for k in range(1, corner_hops):
         z_forward(k)
 
-    att[...] = (acc_s[...] / den_s[...]).astype(jnp.bfloat16)
-
     def att_lanes(i):
         return att_all.at[:, pl.ds(pl.multiple_of((g ^ i) * LANES, LANES), LANES)]
 
@@ -548,24 +597,49 @@
             src_ref=lse_ref.at[g ^ i], dst_ref=lse_all.at[g ^ i], send_sem=l_send.at[i], recv_sem=l_recv.at[i],
             device_id=at(mate(i), tp), device_id_type=MESH)
 
-    for i in range(1, group):
-        att_out(i).start()
+    def split(x):
+        high = x.astype(jnp.bfloat16)
+        return [high, (x - high.astype(jnp.float32)).astype(jnp.bfloat16)]
+
+    def finish(index, carry):
+        i = lax.rem(index + 1, group)
+        block = g ^ i
+        for k in range(2):
+            start = block * rows + k * half
+            at_run = pl.ds(pl.multiple_of(start // wide, run), run)
+            here = pl.ds(pl.multiple_of(start, half), half)
+            terms = split(out_cls[:, at_run, :].reshape(half, LANES)) + split(lse_cls[:, at_run, :].reshape(half, LANES))
+            back_in_order = jnp.dot(turn[1], jnp.concatenate(terms, axis=1), preferred_element_type=jnp.float32)
+            out = back_in_order[:, :LANES] + back_in_order[:, LANES : 2 * LANES]
+            lse = back_in_order[:, 2 * LANES : 3 * LANES] + back_in_order[:, 3 * LANES :]
+            was = top_s[here, :]
+            new = jnp.maximum(was, lse)
+            old_scale, scale = jnp.exp(was - new), jnp.exp(lse - new)
+            den = den_s[here, :] * old_scale + scale
+            att[here, :] = ((acc_s[here, :] * old_scale + out * scale) / den).astype(jnp.bfloat16)
+            lse = new + jnp.log(den)
+            for t in range(half // LANES):
+                columns = lse[t * LANES : (t + 1) * LANES].T
+                off = k * half + t * LANES
+                for h in range(heads):
+                    lse_ref[block, h : h + 1, off : off + LANES] = columns[h * HEAD_SIZE : h * HEAD_SIZE + 1, :]
+
+        @pl.when(i > 0)
+        def _():
+            att_out(i).start()
+            lse_out(i).start()
+
+        return carry
+
+    lax.fori_loop(0, group, finish, 0)
     own_a = pltpu.make_async_copy(att.at[pl.ds(pl.multiple_of(g * rows, rows), rows)], att_lanes(0), own_sem.at[1])
     own_a.start()
+    own_l = pltpu.make_async_copy(lse_ref.at[g], lse_all.at[g], own_sem.at[2])
+    own_l.start()
     for m in early:
         edges(m)
-
-    for t in range(own // LANES):
-        at_rows = pl.ds(t * LANES, LANES)
-        lse = (top_s[at_rows, :] + jnp.log(den_s[at_rows, :])).T
-        b, off = (t * LANES) // rows, (t * LANES) % rows
-        for h in range(heads):
-            lse_ref[b, h : h + 1, off : off + LANES] = lse[h * HEAD_SIZE : h * HEAD_SIZE + 1, :]
-    for i in range(1, group):
-        lse_out(i).start()
-    own_l = pltpu.make_async_copy(lse_ref.at[g], lse_all.at[g], own_sem.at[2])
-    own_l.start()
-
+    for m in late:
+        sides(m)
     own_a.wait()
     for i in range(1, group):
         att_in(i).wait_recv()
@@ -611,6 +685,7 @@
         if m > 1 and m == strips[2] and corner_hops > 1:
             z_relayed(2)
 
+    lag = 3
     for c in range(chunks):
         if by_plane:
             m, side = strips[c // per_strip], c % per_strip
@@ -620,9 +695,10 @@
             if side == per_strip - 1:
                 edges_arrive_late(m)
         multiply(c)
-        if c > 0:
-            add_up(c - 1)
-    add_up(chunks - 1)
+        if c >= lag:
+            add_up(c - lag)
+    for c in range(max(chunks - lag, 0), chunks):
+        add_up(c)
 
     own_l.wait()
     for i in range(1, group):
@@ -683,7 +759,8 @@
 
     turned = w_out.T
     cut = w_out.shape[1]
-    behind = far * own
+    wide = dilation_rates[-1]
+    behind = KEYS_BEHIND * dilation_rates[-2]
     chunks = planes * (2 if group == 4 and 2 * cut % LANES == 0 else 1) if group > 1 else (4 if (n * cut) % (4 * LANES) == 0 else 1)
     chunk = n * cut // chunks
 
@@ -705,6 +782,10 @@
             VMEM((own, 2 * LANES), bf16), VMEM((far, own, 2 * LANES), bf16),
             VMEM((n * cut, width), bf16),
             VMEM((own, LANES), f32), VMEM((behind + own, LANES), f32), VMEM((behind + own, LANES), f32),
+            VMEM((wide, own // wide, LANES), bf16),
+            VMEM((wide, (far + 1) * own // wide, LANES), bf16), VMEM((wide, (far + 1) * own // wide, LANES), bf16),
+            VMEM((wide, own // wide, LANES), f32), VMEM((wide, own // wide, LANES), f32),
+            VMEM((2, rows // 2, rows // 2), bf16),
             VMEM((1 + len(dilation_rates), KEYS_BEHIND, 2 * KEYS_BEHIND), f32),
             VMEM((own, LANES), f32), VMEM((own, LANES), f32), VMEM((own, LANES), f32),
             VMEM((own, LANES), bf16), VMEM((group, heads, rows), f32), VMEM((group, heads, rows), f32),

time: 106 us -> 105 us (level)
  the two profiles are of different devices: /device:TPU:0 before, /device:TPU:25 now
where the time goes in v4:
time: 105 us
  Pallas kernels  102 us (97%)
  local copies, waits for them, and re-layouts  1.75 us (2%)
    pallas_call x1, Pallas kernels, shards(): pl.pallas_call(functools.partial(layer_kernel, n, n_tp, group, far, heads...  102 us

profile of v4, /device:TPU:25, one launch (start us, length us, event | category | flops | bytes accessed | tf_op | source)
XLA Modules:
  0.0 104.7 jit_solution(4218342704158108570)
XLA Ops:
  0.6 102.3 %layer.1 = (bf16[256,3072]{1,0:T(8,128)(2,1)S(1)}, f32[8,512]{1,0:T(8,128)S(1)}) custom-call(bf16[192,512]{1,0:T(8,128)(2,1)} %wq_ref.1, bf16[192,512]{1,0:T(8,128)(2,1)} %wk_ref.1, bf16[192,512]{1,0:T(8,128)(2,1)} %wv_ref.1, bf16[512,3072]{1,0:T(8,128)(2,1)} %tok_ref.1, bf16[192,512]{1,0:T(8,128)(2,1)} %bitcast.1), custom_call_target="tpu_custom_call" | custom-call | flops 4831838208 | bytes 16777216 | tf_op jit(solution)/shard_map/layer/pallas_call | solution.py:770
  102.9 1.1 %copy.9 = bf16[256,3072]{1,0:T(8,128)(2,1)} copy(bf16[256,3072]{1,0:T(8,128)(2,1)S(1)} %get-tuple-element.4) | data formatting | bytes 3145728
  104.1 0.6 copy.10

commit v5 on v4

--- a/solution.py
+++ b/solution.py
@@ -429,32 +429,17 @@
             if k + 1 < planes:
                 o_relay(k + 1)
 
-    tiles(lambda s: (0, s), lambda i, k: None)
-    if group > 1:
-        o_pass(1)
-    if group == 2:
-        tiles(lambda s: (1, s), crossed)
-    if group == 4:
-        tiles(lambda s: (1 + s, 0), crossed)
-        tiles(lambda s: (1 + s, 1), crossed)
-        for s in range(2):
-            for i in near:
-                corner_in(i, s).wait_recv()
-                to_other_cores(3, i - 1, s)
-            crossed(3, s)
-            tile(3, s)
-            if s == 0:
-                o_pass(2)
-
-    by_plane = group > 1
-    def attention(number, begin, end, unroll):
+    def unroll_of(trips):
+        return next(u for u in (3, 2, 5, 1) if trips % u == 0)
+
+    def attention(number, trips, place, opening=False):
         d = dilation_rates[number]
         step = min(KEYS_BEHIND, own // d)
         span = step + KEYS_BEHIND
-        mask_at = 1 + number if begin == 0 else 0
+        mask_at = 1 + number if opening else 0
 
         def block(index, _):
-            cls, b = lax.rem(index, d), index // d
+            cls, b = place(index)
             start = b * (step * d) + cls
             q_at = pl.ds(start, step, stride=d) if d > 1 else pl.ds(pl.multiple_of(start, step), step)
             k_start = behind - KEYS_BEHIND * d + start
@@ -487,8 +472,50 @@
                 acc_s[q_at, :] = acc_s[q_at, :] * old_scale + o * scale
             return _
 
-        lax.fori_loop(begin * d, end * d, block, 0, unroll=unroll)
-
+        lax.fori_loop(0, trips, block, 0, unroll=unroll_of(trips))
+
+    ahead = group == 4 and rows == KEYS_BEHIND * dilation_rates[1]
+    per = rows // KEYS_BEHIND
+    ready_row = 1 + 2 * (g // 2)
+
+    def early_near(u):
+        return 0, jnp.where(u < 9, (g ^ (u // 3)) * per + 1 + lax.rem(u, 3), per * ready_row)
+
+    def late_near(u):
+        rest = jnp.where(u == 3, 2, 4 - ready_row)
+        return 0, jnp.where(u < 3, (g ^ 3) * per + 1 + u, per * rest)
+
+    def early_middle(u):
+        return u, ready_row
+
+    def late_middle(u):
+        return lax.rem(u, 4), jnp.where(u < 4, 2, 4 - ready_row)
+
+    tiles(lambda s: (0, s), lambda i, k: None)
+    if group > 1:
+        o_pass(1)
+    if group == 2:
+        tiles(lambda s: (1, s), crossed)
+    if group == 4:
+        tiles(lambda s: (1 + s, 0), crossed)
+        tiles(lambda s: (1 + s, 1), crossed)
+        if ahead:
+            attention(0, 10, early_near)
+        for s in range(2):
+            for i in near:
+                corner_in(i, s).wait_recv()
+                to_other_cores(3, i - 1, s)
+            if s == 0:
+                if ahead:
+                    attention(1, 4, early_middle)
+            crossed(3, s)
+            tile(3, s)
+            if s == 0 and 2 < planes:
+                o_relayed(2)
+        if 3 < planes:
+            o_relay(3)
+
+    by_plane = group > 1
     def wide_attention(cls, _):
         step = own // wide
         span = step + KEYS_BEHIND
@@ -512,13 +539,7 @@
 
     counts = [own // d // min(KEYS_BEHIND, own // d) for d in dilation_rates[:-1]]
 
-    def unroll_of(trips):
-        return next(u for u in (2, 3, 1) if trips % u == 0)
-
     strips = list(range(planes)) if by_plane else []
-    if 0 < corner_hops < planes - 1:
-        strips.remove(corner_hops)
-        strips.append(corner_hops)
     early, late = strips[1:3], strips[3:]
 
     def later(k, _):
@@ -526,53 +547,54 @@
         when(k + 1 < planes, lambda: o_relay(k + 1))
         return _
 
-    def before_second():
+    def spread_first():
         if by_plane:
             edges(0)
-            for m in early[:1]:
+            for m in early:
                 sides(m)
 
-    def before_halo():
+    def spread_rest():
         started = {1: 1, 2: 2, 4: 3}[group]
         if started < planes:
             lax.fori_loop(started, planes, later, 0)
-        for m in early[1:]:
+        for m in late:
             sides(m)
-        edges_arrive(0)
-        if corner_hops > 0:
-            z_relay(1)
+
+    def sort(h):
+        def unit(u, carry):
+            i, k = u // 2, lax.rem(u, 2)
+            halo_out(h, i, k).wait_recv()
+            start = (g ^ i) * rows + k * half
+            by_class = by_classes(halo_ref[far - h, pl.ds(pl.multiple_of(start, half), half), :])
+            at_run = pl.ds(pl.multiple_of((far - h) * (own // wide) + start // wide, run), run)
+            k_cls[:, at_run, :] = by_class[:, :, :LANES]
+            v_cls[:, at_run, :] = by_class[:, :, LANES:]
+            return carry
+
+        lax.fori_loop(0, 2 * group, unit, 0)
+        if h == 1:
+            ks[:behind] = halo_ref[far - 1, own - behind :, :LANES].astype(jnp.float32)
+            vs[:behind] = halo_ref[far - 1, own - behind :, LANES:].astype(jnp.float32)
+
+    if ahead:
+        attention(0, 5, late_near)
+    else:
+        for number, d in enumerate(dilation_rates[:-1]):
+            if counts[number] > 1:
+                attention(number, (counts[number] - 1) * d, lambda u, d=d: (lax.rem(u, d), 1 + u // d))
+    spread_first()
+    if ahead:
+        attention(1, 8, late_middle)
+    for h in range(1, far + 1):
+        when(plane - h >= 0, functools.partial(sort, h))
 
     for number, d in enumerate(dilation_rates[:-1]):
-        if counts[number] > 1:
-            attention(number, 1, counts[number], unroll_of((counts[number] - 1) * d))
-        if number == 0:
-            before_second()
-    before_halo()
-
-    for h in range(1, far + 1):
-        @pl.when(plane - h >= 0)
-        def _():
-            def sort(u, _):
-                i, k = u // 2, lax.rem(u, 2)
-                halo_out(h, i, k).wait_recv()
-                start = (g ^ i) * rows + k * half
-                by_class = by_classes(halo_ref[far - h, pl.ds(pl.multiple_of(start, half), half), :])
-                at_run = pl.ds(pl.multiple_of((far - h) * (own // wide) + start // wide, run), run)
-                k_cls[:, at_run, :] = by_class[:, :, :LANES]
-                v_cls[:, at_run, :] = by_class[:, :, LANES:]
-                return _
-
-            lax.fori_loop(0, 2 * group, sort, 0)
-            if h == 1:
-                ks[:behind] = halo_ref[far - 1, own - behind :, :LANES].astype(jnp.float32)
-                vs[:behind] = halo_ref[far - 1, own - behind :, LANES:].astype(jnp.float32)
-
-    for number, d in enumerate(dilation_rates[:-1]):
-        attention(number, 0, 1, unroll_of(d))
-    lax.fori_loop(0, wide, wide_attention, 0, unroll=2)
-    for k in range(1, corner_hops):
-        z_forward(k)
-
+        attention(number, d, lambda u: (u, 0), opening=True)
+    edges_arrive(0)
+    if corner_hops > 0:
+        z_relay(1)
+    lax.fori_loop(0, wide, wide_attention, 0, unroll=4)
+    spread_rest()
     def att_lanes(i):
         return att_all.at[:, pl.ds(pl.multiple_of((g ^ i) * LANES, LANES), LANES)]
 
@@ -638,8 +660,10 @@
     own_l.start()
     for m in early:
         edges(m)
+    for k in range(1, corner_hops):
+        z_forward(k)
     for m in late:
-        sides(m)
+        edges(m)
     own_a.wait()
     for i in range(1, group):
         att_in(i).wait_recv()
@@ -689,9 +713,6 @@
     for c in range(chunks):
         if by_plane:
             m, side = strips[c // per_strip], c % per_strip
-            if side == 0:
-                if m in late:
-                    edges(m)
             if side == per_strip - 1:
                 edges_arrive_late(m)
         multiply(c)

time: 105 us -> 103 us (0.981)
  the two profiles are of different devices: /device:TPU:25 before, /device:TPU:0 now
where the time goes in v5:
time: 103 us
  Pallas kernels  100 us (97%)
  local copies, waits for them, and re-layouts  1.75 us (2%)
    pallas_call x1, Pallas kernels, shards(): pl.pallas_call(functools.partial(layer_kernel, n, n_tp, group, far, heads...  100 us

profile of v5, /device:TPU:0, one launch (start us, length us, event | category | flops | bytes accessed | tf_op | source)
XLA Modules:
  0.0 102.6 jit_solution(13648347464456771430)
XLA Ops:
  0.6 100.2 %layer.1 = (bf16[256,3072]{1,0:T(8,128)(2,1)S(1)}, f32[8,512]{1,0:T(8,128)S(1)}) custom-call(bf16[192,512]{1,0:T(8,128)(2,1)} %wq_ref.1, bf16[192,512]{1,0:T(8,128)(2,1)} %wk_ref.1, bf16[192,512]{1,0:T(8,128)(2,1)} %wv_ref.1, bf16[512,3072]{1,0:T(8,128)(2,1)} %tok_ref.1, bf16[192,512]{1,0:T(8,128)(2,1)} %bitcast.1), custom_call_target="tpu_custom_call" | custom-call | flops 4831838208 | bytes 16777216 | tf_op jit(solution)/shard_map/layer/pallas_call | solution.py:791
  100.9 1.1 %copy.9 = bf16[256,3072]{1,0:T(8,128)(2,1)} copy(bf16[256,3072]{1,0:T(8,128)(2,1)S(1)} %get-tuple-element.4) | data formatting | bytes 3145728
  102.0 0.6 copy.10

commit v6 on v5

--- a/solution.py
+++ b/solution.py
@@ -23,7 +23,7 @@
 
 
 def layer_kernel(
-    n, n_tp, group, far, heads, wq_ref, wk_ref, wv_ref, tok_ref, o_ref, mixed_ref, lse_out_ref,
+    n, n_tp, group, far, heads, sum_pieces, wq_ref, wk_ref, wv_ref, tok_ref, o_ref, mixed_ref, lse_out_ref,
     tok_all, w_all, w_ref, kv_ref, halo_ref, o_all, qs, ks, vs, q_cls, k_cls, v_cls, out_cls, lse_cls, turn, bias,
     top_s, den_s, acc_s, att, lse_ref, lse_all, att_all, sums, sums_in,
     pack_sem, own_sem, w1_send, w1_recv, up_send, up_recv, down_send, down_recv, t_send, t_recv, d_send, d_recv,
@@ -84,7 +84,14 @@
         source = (wq_ref, wk_ref, wv_ref)[t].at[:, pl.ds(pl.multiple_of((g ^ i) * LANES, LANES), LANES)]
         lanes = pl.ds(t * LANES, LANES)
         to = w_all.at[sp, :, lanes] if i == 0 else w_ref.at[i, :, lanes]
-        return pltpu.make_async_copy(source, to, pack_sem.at[t, i])
+        return pltpu.make_async_copy(source, to, pack_sem.at[i])
+
+    def all_of(view, sem):
+        return pltpu.make_async_copy(view, view, sem)
+
+    def packed(i):
+        view = w_all.at[sp] if i == 0 else w_ref.at[i]
+        all_of(view, pack_sem.at[i]).wait()
 
     for i in list(range(1, group)) + [0]:
         for t in range(3):
@@ -95,12 +102,12 @@
 
     def w_in_plane(i):
         return pltpu.make_async_remote_copy(
-            src_ref=w_ref.at[i], dst_ref=w_all.at[sp], send_sem=w1_send.at[i], recv_sem=w1_recv.at[i],
+            src_ref=w_ref.at[i], dst_ref=w_all.at[sp], send_sem=w1_send.at[0], recv_sem=w1_recv.at[i - 1],
             device_id=at(mate(i), tp), device_id_type=MESH)
 
     def w_in_plane_arrives(i):
         return pltpu.make_async_remote_copy(
-            src_ref=w_ref.at[i], dst_ref=w_all.at[mate(i)], send_sem=w1_send.at[i], recv_sem=w1_recv.at[i],
+            src_ref=w_ref.at[i], dst_ref=w_all.at[mate(i)], send_sem=w1_send.at[0], recv_sem=w1_recv.at[i - 1],
             device_id=at(mate(i), tp), device_id_type=MESH)
 
     def slab(p, i):
@@ -108,24 +115,24 @@
 
     def up(i, k, p):
         return pltpu.make_async_remote_copy(
-            src_ref=slab(p, i), dst_ref=slab(p, i), send_sem=up_send.at[i, k], recv_sem=up_recv.at[i, k],
+            src_ref=slab(p, i), dst_ref=slab(p, i), send_sem=up_send.at[k - 1], recv_sem=up_recv.at[i, k - 1],
             device_id=at(above, tp), device_id_type=MESH)
 
     def down(i, k, p):
         return pltpu.make_async_remote_copy(
-            src_ref=slab(p, i), dst_ref=slab(p, i), send_sem=down_send.at[i, k], recv_sem=down_recv.at[i, k],
+            src_ref=slab(p, i), dst_ref=slab(p, i), send_sem=down_send.at[k - 1], recv_sem=down_recv.at[i, k - 1],
             device_id=at(below, tp), device_id_type=MESH)
 
     def o_up(k, p):
         ref = strip(lax.rem(p + 2 * planes, planes), 0)
         return pltpu.make_async_remote_copy(
-            src_ref=ref, dst_ref=ref, send_sem=ou_send.at[k], recv_sem=ou_recv.at[k],
+            src_ref=ref, dst_ref=ref, send_sem=ou_send.at[k - 1], recv_sem=ou_recv.at[k - 1],
             device_id=at(above, tp), device_id_type=MESH)
 
     def o_down(k, p):
         ref = strip(lax.rem(p + 2 * planes, planes), 0)
         return pltpu.make_async_remote_copy(
-            src_ref=ref, dst_ref=ref, send_sem=od_send.at[k], recv_sem=od_recv.at[k],
+            src_ref=ref, dst_ref=ref, send_sem=od_send.at[k - 1], recv_sem=od_recv.at[k - 1],
             device_id=at(below, tp), device_id_type=MESH)
 
     def when(condition, action):
@@ -143,9 +150,10 @@
         when(plane - k >= 0, lambda: up(i, k, plane - k).wait_recv())
         when(plane + k < planes, lambda: down(i, k, plane + k).wait_recv())
 
-    def relay_left(k, i):
-        when(~last & (plane - k + 1 >= 0), lambda: up(i, k, plane - k + 1).wait_send())
-        when(~first & (plane + k - 1 < planes), lambda: down(i, k, plane + k - 1).wait_send())
+    def relay_left(k):
+        slabs_of_a_plane = w_all.at[pl.ds(0, group)]
+        when(~last & (plane - k + 1 >= 0), lambda: all_of(slabs_of_a_plane, up_send.at[k - 1]).wait())
+        when(~first & (plane + k - 1 < planes), lambda: all_of(slabs_of_a_plane, down_send.at[k - 1]).wait())
 
     def o_relay(k):
         when(~last & (plane - k + 1 >= 0), lambda: o_up(k, plane - k + 1).start())
@@ -169,69 +177,78 @@
         zigzag = plane + (m // 2 if m % 2 == 0 else -((m + 1) // 2))
         return jnp.where(m <= 2 * short, zigzag, jnp.where(left < right, m, planes - 1 - m))
 
-    def back(q):
-        return lax.rem(plane - q + planes, planes)
-
-    def side_out(q, i):
-        k = back(q)
-        return pltpu.make_async_remote_copy(
-            src_ref=strip(q, 0), dst_ref=strip(q, 0), send_sem=b_send.at[k, i], recv_sem=b_recv.at[k, i],
+    def side_out(m, i):
+        ref = strip(nearest(m), 0)
+        return pltpu.make_async_remote_copy(
+            src_ref=ref, dst_ref=ref, send_sem=b_send.at[0], recv_sem=b_recv.at[m, i - 1],
             device_id=at(mate(i), tp), device_id_type=MESH)
 
-    def side_in(q, i):
-        k = back(q)
-        return pltpu.make_async_remote_copy(
-            src_ref=strip(q, i), dst_ref=strip(q, i), send_sem=b_send.at[k, i], recv_sem=b_recv.at[k, i],
+    def side_in(m, i):
+        ref = strip(nearest(m), i)
+        return pltpu.make_async_remote_copy(
+            src_ref=ref, dst_ref=ref, send_sem=b_send.at[0], recv_sem=b_recv.at[m, i - 1],
             device_id=at(mate(i), tp), device_id_type=MESH)
 
-    def edge_out(q, i):
-        k = back(q)
-        return pltpu.make_async_remote_copy(
-            src_ref=strip(q, i, i - 1), dst_ref=strip(q, i, i - 1), send_sem=c_send.at[k, i], recv_sem=c_recv.at[k, i],
+    up_hops = min(2, planes - 1) if group == 4 else 0
+    down_hops = min(3, planes - 1) if group == 4 else 0
+    z_hops = max(up_hops, down_hops)
+    z_least = min(up_hops, down_hops)
+
+    def edge_at(m):
+        return max(m - z_least, 0)
+
+    def edge_out(m, i):
+        ref = strip(nearest(m), i, i - 1)
+        return pltpu.make_async_remote_copy(
+            src_ref=ref, dst_ref=ref, send_sem=c_send.at[edge_at(m)], recv_sem=c_recv.at[edge_at(m), i - 1],
             device_id=at(mate(3 - i), tp), device_id_type=MESH)
 
-    def edge_in(q, i):
-        k = back(q)
-        return pltpu.make_async_remote_copy(
-            src_ref=strip(q, 3, i - 1), dst_ref=strip(q, 3, i - 1), send_sem=c_send.at[k, i], recv_sem=c_recv.at[k, i],
+    def edge_in(m, i):
+        ref = strip(nearest(m), 3, i - 1)
+        return pltpu.make_async_remote_copy(
+            src_ref=ref, dst_ref=ref, send_sem=c_send.at[edge_at(m)], recv_sem=c_recv.at[edge_at(m), i - 1],
             device_id=at(mate(3 - i), tp), device_id_type=MESH)
 
     def sides(m):
         for i in near:
-            side_out(nearest(m), i).start()
-
-    corner_hops = min(2, planes - 1) if group == 4 else 0
+            side_out(m, i).start()
 
     def edge_goes(m, action):
         if group == 4:
             if m == 0:
                 action()
-            elif m > corner_hops:
-                when(jnp.abs(nearest(m) - plane) > corner_hops, action)
+            elif m > z_least:
+                q = nearest(m)
+                when((plane - q > up_hops) | (q - plane > down_hops), action)
 
     def edges(m):
         for i in near:
-            side_in(nearest(m), i).wait_recv()
-        edge_goes(m, lambda: [edge_out(nearest(m), i).start() for i in near])
+            side_in(m, i).wait_recv()
+        edge_goes(m, lambda: [edge_out(m, i).start() for i in near])
 
     def edges_arrive(m):
-        edge_goes(m, lambda: [edge_in(nearest(m), i).wait_recv() for i in near])
+        edge_goes(m, lambda: [edge_in(m, i).wait_recv() for i in near])
+
+    def edges_left(m):
+        edge_goes(m, lambda: all_of(strip(0, 0), c_send.at[edge_at(m)]).wait())
 
     def z_up(k, p):
         ref = strip(lax.rem(p + 2 * planes, planes), 3)
         return pltpu.make_async_remote_copy(
-            src_ref=ref, dst_ref=ref, send_sem=zu_send.at[k], recv_sem=zu_recv.at[k],
+            src_ref=ref, dst_ref=ref, send_sem=zu_send.at[k - 1], recv_sem=zu_recv.at[k - 1],
             device_id=at(above, tp), device_id_type=MESH)
 
     def z_down(k, p):
         ref = strip(lax.rem(p + 2 * planes, planes), 3)
         return pltpu.make_async_remote_copy(
-            src_ref=ref, dst_ref=ref, send_sem=zd_send.at[k], recv_sem=zd_recv.at[k],
+            src_ref=ref, dst_ref=ref, send_sem=zd_send.at[k - 1], recv_sem=zd_recv.at[k - 1],
             device_id=at(below, tp), device_id_type=MESH)
 
     def z_relay(k):
-        when(~last & (plane - k + 1 >= 0), lambda: z_up(k, plane - k + 1).start())
-        when(~first & (plane + k - 1 < planes), lambda: z_down(k, plane + k - 1).start())
+        if k <= up_hops:
+            when(~last & (plane - k + 1 >= 0), lambda: z_up(k, plane - k + 1).start())
+        if k <= down_hops:
+            when(~first & (plane + k - 1 < planes), lambda: z_down(k, plane + k - 1).start())
 
     def z_forward(k):
         def up_on():
@@ -242,17 +259,24 @@
             z_down(k, plane + k).wait_recv()
             z_down(k + 1, plane + k).start()
 
-        when(~last & (plane - k >= 0), up_on)
-        when(~first & (plane + k < planes), down_on)
+        if k < up_hops:
+            when(~last & (plane - k >= 0), up_on)
+        if k < down_hops:
+            when(~first & (plane + k < planes), down_on)
 
     def z_relayed(k):
-        ends = (True, True) if k == corner_hops else (last, first)
-        when(ends[0] & (plane - k >= 0), lambda: z_up(k, plane - k).wait_recv())
-        when(ends[1] & (plane + k < planes), lambda: z_down(k, plane + k).wait_recv())
+        if k <= up_hops:
+            ends = last if k < up_hops else True
+            when(ends & (plane - k >= 0), lambda: z_up(k, plane - k).wait_recv())
+        if k <= down_hops:
+            ends = first if k < down_hops else True
+            when(ends & (plane + k < planes), lambda: z_down(k, plane + k).wait_recv())
 
     def z_relay_left(k):
-        when(~last & (plane - k + 1 >= 0), lambda: z_up(k, plane - k + 1).wait_send())
-        when(~first & (plane + k - 1 < planes), lambda: z_down(k, plane + k - 1).wait_send())
+        if k <= up_hops:
+            when(~last & (plane - k + 1 >= 0), lambda: z_up(k, plane - k + 1).wait_send())
+        if k <= down_hops:
+            when(~first & (plane + k - 1 < planes), lambda: z_down(k, plane + k - 1).wait_send())
 
     def o_relayed(k):
         def from_below():
@@ -270,35 +294,29 @@
     def tokens_out(i, p, s):
         return pltpu.make_async_remote_copy(
             src_ref=tok_ref.at[bit(s, p, tp)], dst_ref=tok_all.at[g, bit(s, p, tp)],
-            send_sem=t_send.at[i, p, s], recv_sem=t_recv.at[i, p, s], device_id=at(mate(i), tp), device_id_type=MESH)
+            send_sem=t_send.at[0], recv_sem=t_recv.at[i - 1, p, s], device_id=at(mate(i), tp), device_id_type=MESH)
 
     def tokens_in(i, p, s):
         return pltpu.make_async_remote_copy(
             src_ref=tok_ref.at[bit(s, p, tp)], dst_ref=tok_all.at[g ^ i, bit(s, p, tp)],
-            send_sem=t_send.at[i, p, s], recv_sem=t_recv.at[i, p, s], device_id=at(mate(i), tp), device_id_type=MESH)
+            send_sem=t_send.at[0], recv_sem=t_recv.at[i - 1, p, s], device_id=at(mate(i), tp), device_id_type=MESH)
 
     def corner_out(i, s):
         ref = tok_all.at[g ^ i, bit(s, i - 1, tp)]
         return pltpu.make_async_remote_copy(
-            src_ref=ref, dst_ref=ref, send_sem=d_send.at[i, s], recv_sem=d_recv.at[i, s],
+            src_ref=ref, dst_ref=ref, send_sem=d_send.at[0], recv_sem=d_recv.at[i - 1, s],
             device_id=at(mate(3 - i), tp), device_id_type=MESH)
 
     def corner_in(i, s):
         ref = tok_all.at[g ^ 3, bit(s, i - 1, tp)]
         return pltpu.make_async_remote_copy(
-            src_ref=ref, dst_ref=ref, send_sem=d_send.at[i, s], recv_sem=d_recv.at[i, s],
+            src_ref=ref, dst_ref=ref, send_sem=d_send.at[0], recv_sem=d_recv.at[i - 1, s],
             device_id=at(mate(3 - i), tp), device_id_type=MESH)
 
     def across(i, p, s, j):
         ref = tok_all.at[g ^ i, bit(s, p, tp)]
         return pltpu.make_async_remote_copy(
-            src_ref=ref, dst_ref=ref, send_sem=f_send.at[i, p, s, j], recv_sem=f_recv.at[i, p, s, j],
-            device_id=at(sp, lax.rem(tp + j, n_tp)), device_id_type=MESH)
-
-    def across_in(i, p, s, j):
-        ref = tok_all.at[g ^ i, bit(s, p, lax.rem(tp + n_tp - j, n_tp))]
-        return pltpu.make_async_remote_copy(
-            src_ref=ref, dst_ref=ref, send_sem=f_send.at[i, p, s, j], recv_sem=f_recv.at[i, p, s, j],
+            src_ref=ref, dst_ref=ref, send_sem=f_send.at[j - 1], recv_sem=f_recv.at[i - 1, s, j - 1],
             device_id=at(sp, lax.rem(tp + j, n_tp)), device_id_type=MESH)
 
     def to_other_cores(i, p, s):
@@ -309,11 +327,9 @@
         return step if i == 1 else 1 - step
 
     for i in range(1, group):
-        for t in range(3):
-            pack(t, i).wait()
+        packed(i)
         w_in_plane(i).start()
-    for t in range(3):
-        pack(t, 0).wait()
+    packed(0)
     if planes > 1:
         relay(1, 0)
     for step in range(2):
@@ -379,7 +395,7 @@
         view = pl.ds(pl.multiple_of((g ^ i) * rows + k * half, half), half)
         return pltpu.make_async_remote_copy(
             src_ref=kv_ref.at[view], dst_ref=halo_ref.at[far - h, view],
-            send_sem=h_send.at[h, i, k], recv_sem=h_recv.at[h, i, k],
+            send_sem=h_send.at[h - 1], recv_sem=h_recv.at[h - 1, i, k],
             device_id=at(lax.rem(sp + h * group, n), tp), device_id_type=MESH)
 
     def by_classes(y):
@@ -419,9 +435,8 @@
         lax.fori_loop(0, 2, one, 0)
 
     def crossed(i, k):
-        for p in range(2):
-            for j in range(1, n_tp):
-                across_in(i, p, k, j).wait_recv()
+        for j in range(1, n_tp):
+            all_of(tok_all.at[0, pl.ds(0, 2 * bit_rows)], f_recv.at[i - 1, k, j - 1]).wait()
 
     def o_pass(k):
         if k < planes:
@@ -591,8 +606,7 @@
     for number, d in enumerate(dilation_rates[:-1]):
         attention(number, d, lambda u: (u, 0), opening=True)
     edges_arrive(0)
-    if corner_hops > 0:
-        z_relay(1)
+    z_relay(1)
     lax.fori_loop(0, wide, wide_attention, 0, unroll=4)
     spread_rest()
     def att_lanes(i):
@@ -601,22 +615,22 @@
     def att_out(i):
         mine = pl.ds(pl.multiple_of((g ^ i) * rows, rows), rows)
         return pltpu.make_async_remote_copy(
-            src_ref=att.at[mine], dst_ref=att_lanes(0), send_sem=a_send.at[i], recv_sem=a_recv.at[i],
+            src_ref=att.at[mine], dst_ref=att_lanes(0), send_sem=a_send.at[0], recv_sem=a_recv.at[i - 1],
             device_id=at(mate(i), tp), device_id_type=MESH)
 
     def att_in(i):
         return pltpu.make_async_remote_copy(
-            src_ref=att.at[pl.ds(0, rows)], dst_ref=att_lanes(i), send_sem=a_send.at[i], recv_sem=a_recv.at[i],
+            src_ref=att.at[pl.ds(0, rows)], dst_ref=att_lanes(i), send_sem=a_send.at[0], recv_sem=a_recv.at[i - 1],
             device_id=at(mate(i), tp), device_id_type=MESH)
 
     def lse_out(i):
         return pltpu.make_async_remote_copy(
-            src_ref=lse_ref.at[g ^ i], dst_ref=lse_all.at[g], send_sem=l_send.at[i], recv_sem=l_recv.at[i],
+            src_ref=lse_ref.at[g ^ i], dst_ref=lse_all.at[g], send_sem=l_send.at[0], recv_sem=l_recv.at[i - 1],
             device_id=at(mate(i), tp), device_id_type=MESH)
 
     def lse_in(i):
         return pltpu.make_async_remote_copy(
-            src_ref=lse_ref.at[g ^ i], dst_ref=lse_all.at[g ^ i], send_sem=l_send.at[i], recv_sem=l_recv.at[i],
+            src_ref=lse_ref.at[g ^ i], dst_ref=lse_all.at[g ^ i], send_sem=l_send.at[0], recv_sem=l_recv.at[i - 1],
             device_id=at(mate(i), tp), device_id_type=MESH)
 
     def split(x):
@@ -660,65 +674,66 @@
     own_l.start()
     for m in early:
         edges(m)
-    for k in range(1, corner_hops):
-        z_forward(k)
+    z_forward(1)
     for m in late:
         edges(m)
+    for k in range(2, z_hops):
+        z_forward(k)
     own_a.wait()
     for i in range(1, group):
         att_in(i).wait_recv()
 
-    chunks, chunk = sums.shape[0], sums.shape[2]
-
-    per_strip = chunks // planes if by_plane else 1
+    total_columns = sums.shape[1]
+    if by_plane:
+        strip_columns = group * cut
+        pieces = [(m, 0, strip_columns) for m in strips]
+        if group == 4 and 2 * cut % LANES == 0:
+            pieces = pieces[:-1] + [(strips[-1], side, 2 * cut) for side in range(2)]
+    else:
+        pieces = [(c, 0, total_columns // sum_pieces) for c in range(sum_pieces)]
 
     def columns_of(c):
-        if by_plane:
-            m, side = strips[c // per_strip], c % per_strip
-            side = side ^ (g // (group // per_strip)) if per_strip > 1 else 0
-            return pl.ds(pl.multiple_of((nearest(m) * per_strip + side) * chunk, chunk), chunk)
-        return pl.ds(c * chunk, chunk)
+        m, side, size = pieces[c]
+        if not by_plane:
+            return pl.ds(m * size, size)
+        start = nearest(m) * strip_columns
+        if size < strip_columns:
+            start = start + (side ^ (g // 2)) * size
+        return pl.ds(pl.multiple_of(start, LANES), size)
 
     def rows_of(j):
         return pl.ds(pl.multiple_of(lax.rem(tp + j, n_tp) * part, part), part)
 
     def sum_out(c, j):
         return pltpu.make_async_remote_copy(
-            src_ref=sums.at[c, rows_of(j)], dst_ref=sums_in.at[j, c], send_sem=s_send.at[j, c], recv_sem=s_recv.at[j, c],
+            src_ref=sums.at[rows_of(j), columns_of(c)], dst_ref=sums_in.at[j - 1, :, columns_of(c)],
+            send_sem=s_send.at[j - 1], recv_sem=s_recv.at[j - 1, c],
             device_id=at(sp, lax.rem(tp + j, n_tp)), device_id_type=MESH)
 
     def multiply(c):
         w = o_all[columns_of(c), :]
         product = lax.dot_general(att_all[...], w, (((1,), (1,)), ((), ())), preferred_element_type=jnp.float32)
-        sums[c] = product.astype(jnp.bfloat16)
+        sums[:, columns_of(c)] = product.astype(jnp.bfloat16)
         for j in range(1, n_tp):
             sum_out(c, j).start()
 
     def add_up(c):
-        total = sums[c, rows_of(0), :].astype(jnp.float32)
+        total = sums[rows_of(0), columns_of(c)].astype(jnp.float32)
         for j in range(1, n_tp):
             sum_out(c, j).wait_recv()
-            total += sums_in[j, c].astype(jnp.float32)
+            total += sums_in[j - 1, :, columns_of(c)].astype(jnp.float32)
         mixed_ref[:, columns_of(c)] = total.astype(jnp.bfloat16)
 
-    def edges_arrive_late(m):
-        if m > 0:
-            edges_arrive(m)
-        if m == 1 and corner_hops > 0:
-            z_relayed(1)
-        if m > 1 and m == strips[2] and corner_hops > 1:
-            z_relayed(2)
-
-    lag = 3
-    for c in range(chunks):
-        if by_plane:
-            m, side = strips[c // per_strip], c % per_strip
-            if side == per_strip - 1:
-                edges_arrive_late(m)
+    lag = 2
+    for c, (m, side, size) in enumerate(pieces):
+        if by_plane and (side == 1 or size == strip_columns):
+            if m > 0:
+                edges_arrive(m)
+                z_relayed(m)
         multiply(c)
         if c >= lag:
             add_up(c - lag)
-    for c in range(max(chunks - lag, 0), chunks):
+    for c in range(max(len(pieces) - lag, 0), len(pieces)):
         add_up(c)
 
     own_l.wait()
@@ -727,39 +742,27 @@
     for b in range(group):
         lse_out_ref[b * heads : (b + 1) * heads, :] = lse_all[b]
 
-    for i in range(1, group):
-        w_in_plane(i).wait_send()
-        for k in range(2):
-            for s in range(2):
-                for j in range(1, n_tp):
-                    across(i, k, s, j).wait_send()
-    for i in near:
-        for s in range(2):
-            for p in range(2):
-                tokens_out(i, p, s).wait_send()
-            if group == 4:
-                corner_out(i, s).wait_send()
+    if group > 1:
+        all_of(w_ref.at[pl.ds(1, group - 1)], w1_send.at[0]).wait()
+        for j in range(1, n_tp):
+            all_of(tok_all.at[pl.ds(1, group - 1), pl.ds(0, 4 * bit_rows)], f_send.at[j - 1]).wait()
+        all_of(tok_all.at[pl.ds(0, len(near)), pl.ds(0, 4 * bit_rows)], t_send.at[0]).wait()
+        if group == 4:
+            all_of(tok_all.at[0, pl.ds(0, 4 * bit_rows)], d_send.at[0]).wait()
     if planes > 1:
-        lax.fori_loop(1, planes, hops(relay_left), 0)
+        lax.fori_loop(1, planes, lambda k, _: (relay_left(k), _)[1], 0)
         lax.fori_loop(1, planes, lambda k, _: (o_relay_left(k), _)[1], 0)
     for h in range(1, far + 1):
-        @pl.when(plane + h < planes)
-        def _():
-            for i in range(group):
-                for k in range(2):
-                    halo_out(h, i, k).wait_send()
+        when(plane + h < planes, lambda: all_of(kv_ref, h_send.at[h - 1]).wait())
     for j in range(1, n_tp):
-        for c in range(chunks):
-            sum_out(c, j).wait_send()
-    for i in range(1, group):
-        att_out(i).wait_send()
-        lse_out(i).wait_send()
-    if by_plane:
+        all_of(mixed_ref, s_send.at[j - 1]).wait()
+    if group > 1:
+        all_of(att.at[pl.ds(0, (group - 1) * rows)], a_send.at[0]).wait()
+        all_of(lse_ref.at[pl.ds(0, group - 1)], l_send.at[0]).wait()
+        all_of(o_all.at[pl.ds(0, planes * len(near) * cut)], b_send.at[0]).wait()
         for m in range(planes):
-            for i in near:
-                side_out(nearest(m), i).wait_send()
-            edge_goes(m, lambda m=m: [edge_out(nearest(m), i).wait_send() for i in near])
-        for k in range(1, corner_hops + 1):
+            edges_left(m)
+        for k in range(1, z_hops + 1):
             z_relay_left(k)
 
 
@@ -782,14 +785,16 @@
     cut = w_out.shape[1]
     wide = dilation_rates[-1]
     behind = KEYS_BEHIND * dilation_rates[-2]
-    chunks = planes * (2 if group == 4 and 2 * cut % LANES == 0 else 1) if group > 1 else (4 if (n * cut) % (4 * LANES) == 0 else 1)
-    chunk = n * cut // chunks
+    sum_pieces = 5 if group == 4 else planes if group > 1 else (4 if n * cut % (4 * LANES) == 0 else 1)
+    sum_pieces = max(sum_pieces, planes + 1) if group > 1 else sum_pieces
+    corners = max(planes - min(2, planes - 1), 1) if group == 4 else 1
+    mates, others, hops, near = max(group - 1, 1), max(n_tp - 1, 1), max(planes - 1, 1), max(group // 2, 1)
 
     f32, bf16 = jnp.float32, jnp.bfloat16
     dma = pltpu.SemaphoreType.DMA
     vmem = pl.BlockSpec(memory_space=VMEM)
     mixed, lse = pl.pallas_call(
-        functools.partial(layer_kernel, n, n_tp, group, far, heads),
+        functools.partial(layer_kernel, n, n_tp, group, far, heads, sum_pieces),
         out_shape=(
             jax.ShapeDtypeStruct((part, n * cut), bf16),
             jax.ShapeDtypeStruct((group * heads, rows), f32),
@@ -811,21 +816,21 @@
             VMEM((own, LANES), f32), VMEM((own, LANES), f32), VMEM((own, LANES), f32),
             VMEM((own, LANES), bf16), VMEM((group, heads, rows), f32), VMEM((group, heads, rows), f32),
             VMEM((rows, group * LANES), bf16),
-            VMEM((chunks, rows, chunk), bf16), VMEM((n_tp, chunks, part, chunk), bf16),
-            dma((3, group)), dma((4,)),
-            dma((group,)), dma((group,)),
-            dma((group, planes)), dma((group, planes)),
-            dma((group, planes)), dma((group, planes)),
-            dma((group, 2, 2)), dma((group, 2, 2)),
-            dma((group, 2)), dma((group, 2)),
-            dma((group, 2, 2, n_tp)), dma((group, 2, 2, n_tp)),
-            dma((far + 1, group, 2)), dma((far + 1, group, 2)),
-            dma((planes,)), dma((planes,)), dma((planes,)), dma((planes,)),
-            dma((planes, group)), dma((planes, group)),
-            dma((planes, group)), dma((planes, group)),
-            dma((3,)), dma((3,)), dma((3,)), dma((3,)),
-            dma((group,)), dma((group,)), dma((group,)), dma((group,)),
-            dma((n_tp, chunks)), dma((n_tp, chunks)),
+            VMEM((rows, n * cut), bf16), VMEM((others, part, n * cut), bf16),
+            dma((group,)), dma((4,)),
+            dma((1,)), dma((mates,)),
+            dma((hops,)), dma((group, hops)),
+            dma((hops,)), dma((group, hops)),
+            dma((1,)), dma((near, 2, 2)),
+            dma((1,)), dma((near, 2)),
+            dma((others,)), dma((mates, 2, others)),
+            dma((far,)), dma((far, group, 2)),
+            dma((hops,)), dma((hops,)), dma((hops,)), dma((hops,)),
+            dma((1,)), dma((planes if group > 1 else 1, near)),
+            dma((corners,)), dma((corners, near)),
+            dma((2,)), dma((2,)), dma((3,)), dma((3,)),
+            dma((1,)), dma((mates,)), dma((1,)), dma((mates,)),
+            dma((others,)), dma((others, sum_pieces)),
         ],
         compiler_params=pltpu.CompilerParams(collective_id=0, has_side_effects=True, vmem_limit_bytes=46 << 20),
         cost_estimate=pl.CostEstimate(

time: 103 us -> 99.6 us (0.967)
  Pallas kernels: 100 us -> 97 us
    pallas_call x1, Pallas kernels: 100 us -> 97 us  [shards(): pl.pallas_call(functools.partial(layer_kernel, n, n_tp, group, far, heads...]
where the time goes in v6:
time: 99.6 us; the launch traced here: 99.4 us
  Pallas kernels  97 us (97%)
  local copies, waits for them, and re-layouts  1.75 us (2%)
    pallas_call x1, Pallas kernels, shards(): pl.pallas_call(functools.partial(layer_kernel, n, n_tp, group, far, heads...  97 us

profile of v6, /device:TPU:0, one launch (start us, length us, event | category | flops | bytes accessed | tf_op | source)
XLA Modules:
  0.0 99.4 jit_solution(5158435978399714372)
XLA Ops:
  0.6 97.0 %layer.1 = (bf16[256,3072]{1,0:T(8,128)(2,1)S(1)}, f32[8,512]{1,0:T(8,128)S(1)}) custom-call(bf16[192,512]{1,0:T(8,128)(2,1)} %wq_ref.1, bf16[192,512]{1,0:T(8,128)(2,1)} %wk_ref.1, bf16[192,512]{1,0:T(8,128)(2,1)} %wv_ref.1, bf16[512,3072]{1,0:T(8,128)(2,1)} %tok_ref.1, bf16[192,512]{1,0:T(8,128)(2,1)} %bitcast.1), custom_call_target="tpu_custom_call" | custom-call | flops 4831838208 | bytes 16777216 | tf_op jit(solution)/shard_map/layer/pallas_call | solution.py:796
  97.7 1.1 %copy.9 = bf16[256,3072]{1,0:T(8,128)(2,1)} copy(bf16[256,3072]{1,0:T(8,128)(2,1)S(1)} %get-tuple-element.4) | data formatting | bytes 3145728
  98.8 0.6 copy.10

commit v7 on v6

--- a/solution.py
+++ b/solution.py
@@ -213,18 +213,31 @@
         for i in near:
             side_out(m, i).start()
 
+    def beyond(m):
+        return (plane - nearest(m) > up_hops) | (nearest(m) - plane > down_hops)
+
     def edge_goes(m, action):
         if group == 4:
             if m == 0:
                 action()
             elif m > z_least:
-                q = nearest(m)
-                when((plane - q > up_hops) | (q - plane > down_hops), action)
-
-    def edges(m):
+                when(beyond(m), action)
+
+    def edges_on(m):
         for i in near:
             side_in(m, i).wait_recv()
-        edge_goes(m, lambda: [edge_out(m, i).start() for i in near])
+            if group == 4:
+                edge_out(m, i).start()
+
+    def sides_arrive(m):
+        def wait():
+            for i in near:
+                side_in(m, i).wait_recv()
+
+        if group == 4 and m > z_least:
+            when(~beyond(m), wait)
+        elif m > 0:
+            wait()
 
     def edges_arrive(m):
         edge_goes(m, lambda: [edge_in(m, i).wait_recv() for i in near])
@@ -401,6 +414,19 @@
     def by_classes(y):
         sorted_rows = jnp.dot(turn[0], y, preferred_element_type=jnp.float32).astype(jnp.bfloat16)
         return sorted_rows.reshape(wide, run, y.shape[1])
+
+    def sort_unit(h):
+        def unit(u, carry):
+            i, k = u // 2, lax.rem(u, 2)
+            halo_out(h, i, k).wait_recv()
+            start = (g ^ i) * rows + k * half
+            by_class = by_classes(halo_ref[far - h, pl.ds(pl.multiple_of(start, half), half), :])
+            at_run = pl.ds(pl.multiple_of((far - h) * (own // wide) + start // wide, run), run)
+            k_cls[:, at_run, :] = by_class[:, :, :LANES]
+            v_cls[:, at_run, :] = by_class[:, :, LANES:]
+            return carry
+
+        return unit
 
     def tile(i, k):
         block = g ^ i
@@ -517,6 +543,8 @@
         if ahead:
             attention(0, 10, early_near)
         for s in range(2):
+            if s == 1:
+                when(plane >= 1, lambda: lax.fori_loop(0, 2, sort_unit(1), 0))
             for i in near:
                 corner_in(i, s).wait_recv()
                 to_other_cores(3, i - 1, s)
@@ -564,7 +592,7 @@
 
     def spread_first():
         if by_plane:
-            edges(0)
+            edges_on(0)
             for m in early:
                 sides(m)
 
@@ -573,24 +601,19 @@
         if started < planes:
             lax.fori_loop(started, planes, later, 0)
         for m in late:
-            sides(m)
+            when(relayed_in_plane(m), lambda: sides(m))
+
+    def relayed_in_plane(m):
+        return beyond(m) if group == 4 else plane >= 0
 
     def sort(h):
-        def unit(u, carry):
-            i, k = u // 2, lax.rem(u, 2)
-            halo_out(h, i, k).wait_recv()
-            start = (g ^ i) * rows + k * half
-            by_class = by_classes(halo_ref[far - h, pl.ds(pl.multiple_of(start, half), half), :])
-            at_run = pl.ds(pl.multiple_of((far - h) * (own // wide) + start // wide, run), run)
-            k_cls[:, at_run, :] = by_class[:, :, :LANES]
-            v_cls[:, at_run, :] = by_class[:, :, LANES:]
-            return carry
-
-        lax.fori_loop(0, 2 * group, unit, 0)
+        unit = sort_unit(h)
+        lax.fori_loop(begin if h == 1 else 0, 2 * group, unit, 0)
         if h == 1:
             ks[:behind] = halo_ref[far - 1, own - behind :, :LANES].astype(jnp.float32)
             vs[:behind] = halo_ref[far - 1, own - behind :, LANES:].astype(jnp.float32)
 
+    begin = 2 if group == 4 else 0
     if ahead:
         attention(0, 5, late_near)
     else:
@@ -600,13 +623,17 @@
     spread_first()
     if ahead:
         attention(1, 8, late_middle)
+    def pass_corner():
+        edges_arrive(0)
+        z_relay(1)
+
+    when(last, pass_corner)
     for h in range(1, far + 1):
         when(plane - h >= 0, functools.partial(sort, h))
 
     for number, d in enumerate(dilation_rates[:-1]):
         attention(number, d, lambda u: (u, 0), opening=True)
-    edges_arrive(0)
-    z_relay(1)
+    when(~last, pass_corner)
     lax.fori_loop(0, wide, wide_attention, 0, unroll=4)
     spread_rest()
     def att_lanes(i):
@@ -672,13 +699,11 @@
     own_a.start()
     own_l = pltpu.make_async_copy(lse_ref.at[g], lse_all.at[g], own_sem.at[2])
     own_l.start()
-    for m in early:
-        edges(m)
+    for m in late:
+        when(~relayed_in_plane(m), lambda: sides(m))
     z_forward(1)
     for m in late:
-        edges(m)
-    for k in range(2, z_hops):
-        z_forward(k)
+        edge_goes(m, lambda: edges_on(m))
     own_a.wait()
     for i in range(1, group):
         att_in(i).wait_recv()
@@ -726,11 +751,16 @@
 
     lag = 2
     for c, (m, side, size) in enumerate(pieces):
+        if by_plane and side == 0:
+            sides_arrive(m)
         if by_plane and (side == 1 or size == strip_columns):
             if m > 0:
                 edges_arrive(m)
                 z_relayed(m)
         multiply(c)
+        if c == 0:
+            for k in range(2, z_hops):
+                z_forward(k)
         if c >= lag:
             add_up(c - lag)
     for c in range(max(len(pieces) - lag, 0), len(pieces)):

time: 99.6 us -> 98 us (0.984)
  Pallas kernels: 97 us -> 95.5 us
    pallas_call x1, Pallas kernels: 97 us -> 95.5 us  [shards(): pl.pallas_call(functools.partial(layer_kernel, n, n_tp, group, far, heads...]
where the time goes in v7:
time: 98 us; the launch traced here: 97.9 us
  Pallas kernels  95.5 us (97%)
  local copies, waits for them, and re-layouts  1.75 us (2%)
    pallas_call x1, Pallas kernels, shards(): pl.pallas_call(functools.partial(layer_kernel, n, n_tp, group, far, heads...  95.5 us

profile of v7, /device:TPU:0, one launch (start us, length us, event | category | flops | bytes accessed | tf_op | source)
XLA Modules:
  0.0 97.9 jit_solution(769196507050530107)
XLA Ops:
  0.6 95.5 %layer.1 = (bf16[256,3072]{1,0:T(8,128)(2,1)S(1)}, f32[8,512]{1,0:T(8,128)S(1)}) custom-call(bf16[192,512]{1,0:T(8,128)(2,1)} %wq_ref.1, bf16[192,512]{1,0:T(8,128)(2,1)} %wk_ref.1, bf16[192,512]{1,0:T(8,128)(2,1)} %wv_ref.1, bf16[512,3072]{1,0:T(8,128)(2,1)} %tok_ref.1, bf16[192,512]{1,0:T(8,128)(2,1)} %bitcast.1), custom_call_target="tpu_custom_call" | custom-call | flops 4831838208 | bytes 16777216 | tf_op jit(solution)/shard_map/layer/pallas_call | solution.py:826
  96.1 1.1 %copy.9 = bf16[256,3072]{1,0:T(8,128)(2,1)} copy(bf16[256,3072]{1,0:T(8,128)(2,1)S(1)} %get-tuple-element.4) | data formatting | bytes 3145728
  97.2 0.6 copy.10

commit v8 on v7

--- a/solution.py
+++ b/solution.py
@@ -190,7 +190,8 @@
             device_id=at(mate(i), tp), device_id_type=MESH)
 
     up_hops = min(2, planes - 1) if group == 4 else 0
-    down_hops = min(3, planes - 1) if group == 4 else 0
+    down_hops = up_hops
+    straight = group == 4 and planes - 1 > up_hops
     z_hops = max(up_hops, down_hops)
     z_least = min(up_hops, down_hops)
 
@@ -213,8 +214,21 @@
         for i in near:
             side_out(m, i).start()
 
+    def straight_out():
+        ref = strip(planes - 1, 3)
+        return pltpu.make_async_remote_copy(
+            src_ref=ref, dst_ref=ref, send_sem=zd_send.at[2], recv_sem=zd_recv.at[2],
+            device_id=at(above, tp), device_id_type=MESH)
+
+    def straight_in():
+        ref = strip(planes - 1, 3)
+        return pltpu.make_async_remote_copy(
+            src_ref=ref, dst_ref=ref, send_sem=zd_send.at[2], recv_sem=zd_recv.at[2],
+            device_id=at(below, tp), device_id_type=MESH)
+
     def beyond(m):
-        return (plane - nearest(m) > up_hops) | (nearest(m) - plane > down_hops)
+        there = nearest(m) - plane
+        return (-there > up_hops) | ((there > down_hops) & (there < planes - 1))
 
     def edge_goes(m, action):
         if group == 4:
@@ -471,7 +485,7 @@
                 o_relay(k + 1)
 
     def unroll_of(trips):
-        return next(u for u in (3, 2, 5, 1) if trips % u == 0)
+        return next(u for u in (5, 4, 3, 2, 1) if trips % u == 0)
 
     def attention(number, trips, place, opening=False):
         d = dilation_rates[number]
@@ -625,6 +639,8 @@
         attention(1, 8, late_middle)
     def pass_corner():
         edges_arrive(0)
+        if straight:
+            when(last, lambda: straight_out().start())
         z_relay(1)
 
     when(last, pass_corner)
@@ -757,6 +773,8 @@
             if m > 0:
                 edges_arrive(m)
                 z_relayed(m)
+                if straight and m == planes - 1:
+                    when(first, lambda: straight_in().wait_recv())
         multiply(c)
         if c == 0:
             for k in range(2, z_hops):
@@ -794,6 +812,8 @@
             edges_left(m)
         for k in range(1, z_hops + 1):
             z_relay_left(k)
+        if straight:
+            when(last, lambda: straight_out().wait_send())
 
 
 def shards(n, n_tp, tokens, w_query, w_key, w_value, w_out):

time: 98 us -> 97.9 us (level)
  no operation moved by 1% of the time
where the time goes in v8:
time: 97.9 us; the launch traced here: 97.3 us
  Pallas kernels  94.9 us (97%)
  local copies, waits for them, and re-layouts  1.75 us (2%)
    pallas_call x1, Pallas kernels, shards(): pl.pallas_call(functools.partial(layer_kernel, n, n_tp, group, far, heads...  94.9 us

profile of v8, /device:TPU:0, one launch (start us, length us, event | category | flops | bytes accessed | tf_op | source)
XLA Modules:
  0.0 97.3 jit_solution(14317149333086608134)
XLA Ops:
  0.6 94.9 %layer.1 = (bf16[256,3072]{1,0:T(8,128)(2,1)S(1)}, f32[8,512]{1,0:T(8,128)S(1)}) custom-call(bf16[192,512]{1,0:T(8,128)(2,1)} %wq_ref.1, bf16[192,512]{1,0:T(8,128)(2,1)} %wk_ref.1, bf16[192,512]{1,0:T(8,128)(2,1)} %wv_ref.1, bf16[512,3072]{1,0:T(8,128)(2,1)} %tok_ref.1, bf16[192,512]{1,0:T(8,128)(2,1)} %bitcast.1), custom_call_target="tpu_custom_call" | custom-call | flops 4831838208 | bytes 16777216 | tf_op jit(solution)/shard_map/layer/pallas_call | solution.py:846
  95.5 1.1 %copy.9 = bf16[256,3072]{1,0:T(8,128)(2,1)} copy(bf16[256,3072]{1,0:T(8,128)(2,1)S(1)} %get-tuple-element.4) | data formatting | bytes 3145728
  96.7 0.6 copy.10
